TPU v7x, 128 devices: a whole 4x4x4 slice. The times are simulated.
128 devices in a mesh: sp: 16 (over z, y), dp: 8 (over x, core).
Axes of the slice: x: 4, y: 4, z: 4, core: 2. Of those that a mesh axis runs over, the one named last changes fastest.
Arguments:
- tokens: bfloat16 [8, 4096, 2048], P('dp', 'sp'), may hold values from -6 to 6
- in_gain: float32 [2048], replicated, may hold values from 0.1 to 1.9
- w_query_down: bfloat16 [2048, 512], P('dp'), may hold values from -0.125 to 0.125
- w_latent_down: bfloat16 [2048, 256], P('dp'), may hold values from -0.125 to 0.125
- w_rope_key: bfloat16 [2048, 64], replicated, may hold values from -0.125 to 0.125
- query_latent_gain: float32 [512], replicated, may hold values from 0.1 to 1.9
- latent_gain: float32 [256], replicated, may hold values from 0.1 to 1.9
- w_query_up: bfloat16 [512, 3072], P('dp', 'sp'), may hold values from -0.25 to 0.25
- w_key_up: bfloat16 [256, 2048], P('dp', 'sp'), may hold values from -0.375 to 0.375
- w_value_up: bfloat16 [256, 2048], P('dp', 'sp'), may hold values from -0.375 to 0.375
- query_gain: float32 [192], replicated, may hold values from 0.5 to 14
- key_gain: float32 [192], replicated, may hold values from 0.5 to 14
- out_gain: float32 [2048], replicated, may hold values from 0.1 to 1.9
- w_out: bfloat16 [2048, 2048], P(('sp', 'dp')), may hold values from -0.125 to 0.125
Outputs:
- result: bfloat16 [8, 4096, 2048], P('dp', 'sp')
All inputs are finite; a program needn't handle non-finite values.
Results may differ from a plain program's by a relative error of at most 0.034.
The roundings to bfloat16 on the way count: a program that leaves them out, or rounds other values in their place, can miss the bound.
Values may be sent and summed in bfloat16 or wider, within the bound.
A program may use at most 64 MiB of HBM per device.

v0:
```python
import jax
import jax.numpy as jnp
from jax import lax
from jax.sharding import PartitionSpec as P

HEADS = 16


EPS = 1e-06
THETA = 10000.0
NEG_BIG = -1e30


def in_one_piece(arrays, axis, dim, along):
    ends, at = ([], 0)
    for a in arrays[:-1]:
        at += a.shape[along]
        ends.append(at)
    both = jnp.concatenate(arrays, axis=along)
    return tuple(jnp.split(lax.all_gather(both, axis, axis=dim, tiled=True), ends, axis=along))


def joined_along(blocks, dim):
    dims = list(blocks.shape[1:])
    dims[dim] *= blocks.shape[0]
    return jnp.moveaxis(blocks, 0, dim).reshape(dims)


def sent_to_all(value, axis):
    copies = jnp.broadcast_to(value, (lax.axis_size(axis), *value.shape))
    return lax.all_to_all(copies, axis, split_axis=0, concat_axis=0, tiled=True)


def gathered_copies(value, axis, dim):
    return joined_along(sent_to_all(value, axis), dim)


def rms_scale(values, scaling):
    return values * lax.rsqrt(jnp.mean(values * values, axis=-1, keepdims=True) + EPS) * scaling


def rotate(tail_part, positions):
    half_width = tail_part.shape[-1] // 2
    frequency = THETA ** (-jnp.arange(half_width, dtype=jnp.float32) / half_width)
    angles = positions[:, None] * frequency[None, :]
    cosine = jnp.cos(angles)[:, None, :]
    sine = jnp.sin(angles)[:, None, :]
    first_half = tail_part[..., :half_width]
    second_half = tail_part[..., half_width:]
    return jnp.concatenate(
        [first_half * cosine - second_half * sine, second_half * cosine + first_half * sine],
        axis=-1,
    )


def finish_heads(joined, positions, scaling, rope_width):
    row_count = joined.shape[0]
    normal = rms_scale(joined, scaling)
    turned = rotate(normal[..., -rope_width:], positions)
    return (
        jnp.concatenate([normal[..., :-rope_width], turned], axis=-1)
        .astype(jnp.bfloat16)
        .reshape(row_count, -1)
    )


def make_queries(query_total, positions, scaling, head_count, rope_width):
    row_count = query_total.shape[0]
    return finish_heads(
        query_total.reshape(row_count, head_count, -1), positions, scaling, rope_width
    )


def make_keys(key_total, rope_key, positions, scaling, head_count):
    row_count = key_total.shape[0]
    rope_width = rope_key.shape[1]
    shaped = key_total.reshape(row_count, head_count, -1)
    shared = rope_key.astype(jnp.float32)[:, None, :]
    return finish_heads(jnp.concatenate([shaped, shared], axis=-1), positions, scaling, rope_width)


def single_fold(inputs, piece):
    return jnp.dot(inputs, piece, preferred_element_type=jnp.float32)


def double_fold(inputs, pieces):
    return (
        jnp.dot(inputs, pieces[0], preferred_element_type=jnp.float32),
        jnp.dot(inputs, pieces[1], preferred_element_type=jnp.float32),
    )


def attend(queries, keys, values, head_count):
    length = queries.shape[0]
    block_rows = min(512, length)
    query_blocks = queries.reshape(length // block_rows, block_rows, head_count, -1)
    key_heads = keys.reshape(length, head_count, -1)
    value_heads = values.reshape(length, head_count, -1)
    score_scale = key_heads.shape[-1] ** (-0.5)
    key_pos = jnp.arange(length)

    def one_block(block_args):
        query_block, block_index = block_args
        scores = (
            jnp.einsum("qhd,khd->hqk", query_block, key_heads, preferred_element_type=jnp.float32)
            * score_scale
        )
        query_pos = block_index * block_rows + jnp.arange(block_rows)
        allowed = key_pos[None, :] <= query_pos[:, None]
        scores = jnp.where(allowed[None], scores, NEG_BIG)
        weights = jax.nn.softmax(scores, axis=-1).astype(jnp.bfloat16)
        return jnp.einsum(
            "hqk,khd->qhd", weights, value_heads, preferred_element_type=jnp.float32
        ).astype(jnp.bfloat16)

    outcome = lax.map(one_block, (query_blocks, jnp.arange(length // block_rows)))
    return outcome.reshape(length, -1)


def per_device(
    tokens,
    in_gain,
    w_query_down,
    w_latent_down,
    w_rope_key,
    query_latent_gain,
    latent_gain,
    w_query_up,
    w_key_up,
    w_value_up,
    query_gain,
    key_gain,
    out_gain,
    w_out,
):
    seq_devices = lax.axis_size("sp")
    head_count = HEADS // seq_devices
    own_rows = tokens.shape[1]
    length = own_rows * seq_devices
    rope_width = w_rope_key.shape[1]
    local_rows = tokens.reshape(own_rows, tokens.shape[2])
    normed = rms_scale(local_rows.astype(jnp.float32), in_gain).astype(jnp.bfloat16)
    query_sum, latent_sum = double_fold(
        normed, in_one_piece((w_query_down, w_latent_down), "dp", 0, 1)
    )
    latent_q = rms_scale(query_sum, query_latent_gain).astype(jnp.bfloat16)
    latent_kv = rms_scale(latent_sum, latent_gain).astype(jnp.bfloat16)
    rope_key = jnp.dot(normed, w_rope_key, preferred_element_type=jnp.float32).astype(jnp.bfloat16)
    every_q, every_kv, every_rope = in_one_piece((latent_q, latent_kv, rope_key), "sp", 0, 1)
    positions = jnp.arange(length, dtype=jnp.float32)
    query_total = single_fold(every_q, gathered_copies(w_query_up, "dp", 0))
    key_total, value_total = double_fold(
        every_kv,
        (
            lax.all_gather(w_key_up, "dp", axis=0, tiled=True),
            lax.all_gather(w_value_up, "dp", axis=0, tiled=True),
        ),
    )
    queries = make_queries(query_total, positions, query_gain, head_count, rope_width)
    keys = make_keys(key_total, every_rope, positions, key_gain, head_count)
    values = value_total.astype(jnp.bfloat16)
    attended = attend(queries, keys, values, head_count)
    token_heads = lax.all_to_all(attended, "sp", split_axis=0, concat_axis=1, tiled=True)
    mixed = rms_scale(token_heads.astype(jnp.float32), out_gain).astype(jnp.bfloat16)
    projected = single_fold(mixed, lax.all_gather(w_out, ("sp", "dp"), axis=0, tiled=True))
    return projected.astype(jnp.bfloat16).reshape(1, own_rows, w_out.shape[1])


def solution(mesh):
    in_specs = (
        P("dp", "sp", None),
        P(),
        P("dp", None),
        P("dp", None),
        P(),
        P(),
        P(),
        P("dp", "sp"),
        P("dp", "sp"),
        P("dp", "sp"),
        P(),
        P(),
        P(),
        P(("sp", "dp"), None),
    )
    out_specs = P("dp", "sp", None)
    return jax.shard_map(
        per_device, mesh=mesh, in_specs=in_specs, out_specs=out_specs, check_vma=False
    )
```

profile of v0, /device:TPU:24, one launch (start us, length us, event | category | flops | bytes accessed | tf_op | source)
XLA Modules:
  0.0 223.0 jit_solution(16825096950358641469)
XLA Ops:
  6.5 1.9 pad_maximum_fusion.4
  8.5 1.5 fusion.17
  10.0 1.7 convolution_convert_fusion.2
  11.9 26.9 %all-gather.4.cloned.1.call-done = bf16[2048,768]{1,0:T(8,128)(2,1)} async-done(((bf16[256,768]{1,0:T(8,128)(2,1)}), bf16[2048,768]{1,0:T(8,128)(2,1)}) %all-gather.4.cloned.1.call-update) | async-done | bytes 3145744 | tf_op jit(solution)/shard_map/all_gather | solution.py:20
  38.8 2.4 %multiply_reduce_fusion.2 = (f32[256]{0:T(256)S(1)}, f32[256,512]{1,0:T(8,128)S(1)}) fusion(bf16[2048,768]{1,0:T(8,128)(2,1)} %all-gather.4.cloned.1.call-done, bf16[1,256,2048]{2,1,0:T(8,128)(2,1)S(1)} %copy-done.2, f32[2048]{0:T(1024)S(1)} %copy-done.11, f32[256]{0:T(256)S(1)} %add_rsqrt_fusion.5), kind=kOutput, calls=%fused_computation.61 | convolution fusion | flops 539229952 | bytes 3680256 | tf_op jit(solution)/shard_map/dot_general | solution.py:88
  41.3 1.9 multiply_reduce_fusion.3
  43.6 0.8 pad_maximum_fusion.3
  44.5 0.7 broadcast_in_dim.11
  45.2 4.0 %all-to-all-start = ((bf16[8,64,192]{2,1,0:T(8,128)(2,1)}), bf16[8,64,192]{2,1,0:T(8,128)(2,1)}, u32[]{:S(2)}, u32[]{:S(2)}) async-start(bf16[8,64,192]{2,1,0:T(8,128)(2,1)} %broadcast_in_dim.11), calls=%async_computation | async-start | bytes 524288 | tf_op jit(solution)/shard_map/all_to_all | solution.py:31
  49.3 0.7 all-gather.8.cloned.1.call-update
  50.0 13.8 %all_gather.17 = bf16[256,128]{1,0:T(8,128)(2,1)S(1)} all-gather(bf16[32,128]{1,0:T(8,128)(2,1)S(1)} %copy-done.5), channel_id=1, replica_groups=mesh['sp'=16,'dp'=8] {'dp'}, dimensions={0}, use_global_device_ids=true | all-gather | bytes 73728 | tf_op jit(solution)/shard_map/all_gather | solution.py:155
  63.8 12.9 %all_gather.18 = bf16[256,128]{1,0:T(8,128)(2,1)S(1)} all-gather(bf16[32,128]{1,0:T(8,128)(2,1)S(1)} %copy-done.6), channel_id=1, replica_groups=mesh['sp'=16,'dp'=8] {'dp'}, dimensions={0}, use_global_device_ids=true | all-gather | bytes 73728 | tf_op jit(solution)/shard_map/all_gather | solution.py:156
  76.7 34.1 %all-gather.6.cloned.1.call-done = bf16[4096,832]{1,0:T(8,128)(2,1)} async-done(((bf16[256,832]{1,0:T(8,128)(2,1)}), bf16[4096,832]{1,0:T(8,128)(2,1)}) %all-gather.6.cloned.1.call-update) | async-done | bytes 6815760 | tf_op jit(solution)/shard_map/all_gather | solution.py:20
  110.8 1.4 fusion.26
  112.7 2.4 %convolution_bitcast_fusion = f32[4096,1,128]{0,2,1:T(8,128)S(1)} fusion(bf16[256,128]{1,0:T(8,128)(2,1)S(1)} %all_gather.17, bf16[4096,832]{1,0:T(8,128)(2,1)} %all-gather.6.cloned.1.call-done), kind=kOutput, calls=%fused_computation.16 | convolution fusion | flops 268435456 | bytes 4259840 | tf_op jit(solution)/shard_map/dot_general | solution.py:88
  115.5 3.7 %multiply_reduce_fusion.1 = (f32[4096]{0:T(1024)S(1)}, f32[4096,192]{0,1:T(8,128)S(1)}) fusion(bf16[512,192]{1,0:T(8,128)(2,1)} %bitcast.2, bf16[4096,832]{1,0:T(8,128)(2,1)} %all-gather.6.cloned.1.call-done), kind=kOutput, calls=%fused_computation.25 | convolution fusion | flops 806875136 | bytes 7618560 | tf_op jit(solution)/shard_map/dot_general | solution.py:83
  120.6 2.5 %subtract_convert_fusion = (bf16[4096,1,32]{0,2,1:T(8,128)(2,1)S(1)}, bf16[4096,1,32]{0,2,1:T(8,128)(2,1)S(1)}, bf16[4096,1,32]{0,2,1:T(8,128)(2,1)S(1)}, bf16[4096,1,32]{0,2,1:T(8,128)(2,1)S(1)}) fusion(f32[4096,1,192]{0,2,1:T(8,128)S(1)} %multiply_multiply_fusion, f32[32]{0:T(128)S(1)} %multiply_power_fusion, f32[4096,1,192]{0,2,1:T(8,128)S(1)} %multiply_bitcast_fusion), kind=kLoop, calls=%fused_computation.54 | loop fusion | flops 2228224 | bytes 3145856 | tf_op jit(solution)/shard_map/convert.5
  123.5 3.3 %fusion.12 = bf16[4096,1,128]{2,0,1:T(8,128)(2,1)} fusion(bf16[256,128]{1,0:T(8,128)(2,1)S(1)} %all_gather.18, bf16[4096,832]{1,0:T(8,128)(2,1)} %all-gather.6.cloned.1.call-done), kind=kOutput, calls=%fused_computation.18 | convolution fusion | flops 268959744 | bytes 3211264 | tf_op jit(solution)/shard_map/dot_general | solution.py:89
  126.8 58.7 %while.11 = (s32[]{:T(128)}, bf16[8,512,1,128]{3,1,2,0:T(8,128)(2,1)}, s32[8]{0:T(128)S(1)}, bf16[8,512,1,192]{1,3,2,0:T(8,128)(2,1)S(1)}, bf16[4096,1,192]{0,2,...) while((s32[]{:T(128)}, bf16[8,512,1,128]{3,1,2,0:T(8,128)(2,1)}, ...), condition=%wide.region_8.9_spmd.clone, body=%wide.region_5.8_spmd.clone.sunk | while | flops 1361116672 | bytes 32324240 | solution.py:116
  126.8 0.6 dynamic_slice.19
  128.1 1.9 fusion.46
  130.0 1.3 fusion.47
  131.3 2.8 %fusion.48 = bf16[8,512,1,128]{3,1,2,0:T(8,128)(2,1)} fusion(bf16[8,512,1,128]{3,1,2,0:T(8,128)(2,1)} %get-tuple-element.141, s32[]{:T(128)} %get-tuple-element.140, f32[512,4096]{1,0:T(8,128)S(1)} %get-tuple-element.130, f32[512]{0:T(512)S(1)} %fusion.47, f32[512]{0:T(512)S(1)} %get-tuple-element.131, bf16[4096,1,128]{2,0,1:T(8,128)(2,1)S(1)} %copy-done.1), kind=kOutput, calls=%fused_computation.10.clone.1 | convolution fusion | flops 543227904 | bytes 9572864 | tf_op jit(solution)/shard_map/while/body/eval_jaxpr/hqk,khd->qhd/dot_general | solution.py:112
  135.4 2.0 fusion.46
  137.4 1.3 fusion.47
  138.7 2.8 %fusion.48 = bf16[8,512,1,128]{3,1,2,0:T(8,128)(2,1)} fusion(bf16[8,512,1,128]{3,1,2,0:T(8,128)(2,1)} %get-tuple-element.141, s32[]{:T(128)} %get-tuple-element.140, f32[512,4096]{1,0:T(8,128)S(1)} %get-tuple-element.130, f32[512]{0:T(512)S(1)} %fusion.47, f32[512]{0:T(512)S(1)} %get-tuple-element.131, bf16[4096,1,128]{2,0,1:T(8,128)(2,1)S(1)} %copy-done.1), kind=kOutput, calls=%fused_computation.10.clone.1 | convolution fusion | flops 543227904 | bytes 9572864 | tf_op jit(solution)/shard_map/while/body/eval_jaxpr/hqk,khd->qhd/dot_general | solution.py:112
  142.7 2.0 fusion.46
  144.7 1.3 fusion.47
  146.0 2.8 %fusion.48 = bf16[8,512,1,128]{3,1,2,0:T(8,128)(2,1)} fusion(bf16[8,512,1,128]{3,1,2,0:T(8,128)(2,1)} %get-tuple-element.141, s32[]{:T(128)} %get-tuple-element.140, f32[512,4096]{1,0:T(8,128)S(1)} %get-tuple-element.130, f32[512]{0:T(512)S(1)} %fusion.47, f32[512]{0:T(512)S(1)} %get-tuple-element.131, bf16[4096,1,128]{2,0,1:T(8,128)(2,1)S(1)} %copy-done.1), kind=kOutput, calls=%fused_computation.10.clone.1 | convolution fusion | flops 543227904 | bytes 9572864 | tf_op jit(solution)/shard_map/while/body/eval_jaxpr/hqk,khd->qhd/dot_general | solution.py:112
  150.1 2.0 fusion.46
  152.0 1.3 fusion.47
  153.3 2.8 %fusion.48 = bf16[8,512,1,128]{3,1,2,0:T(8,128)(2,1)} fusion(bf16[8,512,1,128]{3,1,2,0:T(8,128)(2,1)} %get-tuple-element.141, s32[]{:T(128)} %get-tuple-element.140, f32[512,4096]{1,0:T(8,128)S(1)} %get-tuple-element.130, f32[512]{0:T(512)S(1)} %fusion.47, f32[512]{0:T(512)S(1)} %get-tuple-element.131, bf16[4096,1,128]{2,0,1:T(8,128)(2,1)S(1)} %copy-done.1), kind=kOutput, calls=%fused_computation.10.clone.1 | convolution fusion | flops 543227904 | bytes 9572864 | tf_op jit(solution)/shard_map/while/body/eval_jaxpr/hqk,khd->qhd/dot_general | solution.py:112
  157.4 2.0 fusion.46
  159.4 1.3 fusion.47
  160.7 2.8 %fusion.48 = bf16[8,512,1,128]{3,1,2,0:T(8,128)(2,1)} fusion(bf16[8,512,1,128]{3,1,2,0:T(8,128)(2,1)} %get-tuple-element.141, s32[]{:T(128)} %get-tuple-element.140, f32[512,4096]{1,0:T(8,128)S(1)} %get-tuple-element.130, f32[512]{0:T(512)S(1)} %fusion.47, f32[512]{0:T(512)S(1)} %get-tuple-element.131, bf16[4096,1,128]{2,0,1:T(8,128)(2,1)S(1)} %copy-done.1), kind=kOutput, calls=%fused_computation.10.clone.1 | convolution fusion | flops 543227904 | bytes 9572864 | tf_op jit(solution)/shard_map/while/body/eval_jaxpr/hqk,khd->qhd/dot_general | solution.py:112
  164.7 2.0 fusion.46
  166.7 1.3 fusion.47
  168.0 2.8 %fusion.48 = bf16[8,512,1,128]{3,1,2,0:T(8,128)(2,1)} fusion(bf16[8,512,1,128]{3,1,2,0:T(8,128)(2,1)} %get-tuple-element.141, s32[]{:T(128)} %get-tuple-element.140, f32[512,4096]{1,0:T(8,128)S(1)} %get-tuple-element.130, f32[512]{0:T(512)S(1)} %fusion.47, f32[512]{0:T(512)S(1)} %get-tuple-element.131, bf16[4096,1,128]{2,0,1:T(8,128)(2,1)S(1)} %copy-done.1), kind=kOutput, calls=%fused_computation.10.clone.1 | convolution fusion | flops 543227904 | bytes 9572864 | tf_op jit(solution)/shard_map/while/body/eval_jaxpr/hqk,khd->qhd/dot_general | solution.py:112
  172.1 2.0 fusion.46
  174.0 1.3 fusion.47
  175.4 2.8 %fusion.48 = bf16[8,512,1,128]{3,1,2,0:T(8,128)(2,1)} fusion(bf16[8,512,1,128]{3,1,2,0:T(8,128)(2,1)} %get-tuple-element.141, s32[]{:T(128)} %get-tuple-element.140, f32[512,4096]{1,0:T(8,128)S(1)} %get-tuple-element.130, f32[512]{0:T(512)S(1)} %fusion.47, f32[512]{0:T(512)S(1)} %get-tuple-element.131, bf16[4096,1,128]{2,0,1:T(8,128)(2,1)S(1)} %copy-done.1), kind=kOutput, calls=%fused_computation.10.clone.1 | convolution fusion | flops 543227904 | bytes 9572864 | tf_op jit(solution)/shard_map/while/body/eval_jaxpr/hqk,khd->qhd/dot_general | solution.py:112
  179.5 2.0 fusion.46
  181.4 1.3 fusion.47
  182.7 2.8 %fusion.48 = bf16[8,512,1,128]{3,1,2,0:T(8,128)(2,1)} fusion(bf16[8,512,1,128]{3,1,2,0:T(8,128)(2,1)} %get-tuple-element.141, s32[]{:T(128)} %get-tuple-element.140, f32[512,4096]{1,0:T(8,128)S(1)} %get-tuple-element.130, f32[512]{0:T(512)S(1)} %fusion.47, f32[512]{0:T(512)S(1)} %get-tuple-element.131, bf16[4096,1,128]{2,0,1:T(8,128)(2,1)S(1)} %copy-done.1), kind=kOutput, calls=%fused_computation.10.clone.1 | convolution fusion | flops 543227904 | bytes 9572864 | tf_op jit(solution)/shard_map/while/body/eval_jaxpr/hqk,khd->qhd/dot_general | solution.py:112
  185.6 20.0 %all_to_all.18 = bf16[16,256,128]{2,1,0:T(8,128)(2,1)S(1)} all-to-all(bf16[16,256,128]{2,1,0:T(8,128)(2,1)} %bitcast.7), channel_id=1, replica_groups=mesh['sp'=16,'dp'=8] {'sp'}, dimensions={0} | all-to-all | bytes 2097152 | tf_op jit(solution)/shard_map/all_to_all | solution.py:163
  205.6 1.6 convert_bitcast_fusion
  207.1 1.9 copy.42
  209.8 6.7 %fusion.15 = bf16[1,256,2048]{2,1,0:T(8,128)(2,1)} fusion(bf16[256,2048]{0,1:T(8,128)(2,1)S(1)} %fusion.23, bf16[2048,2048]{1,0:T(8,128)(2,1)} %all-gather.8.cloned.1.call-done), kind=kOutput, calls=%fused_computation.31 | convolution fusion | flops 2148007936 | bytes 10485760 | tf_op jit(solution)/shard_map/dot_general | solution.py:83
  (85 shorter events, 8.2 us)
Async XLA Ops:
  6.5 3.5 %copy-start = (bf16[2048,64]{0,1:T(8,128)(2,1)S(1)}, bf16[2048,64]{0,1:T(8,128)(2,1)}, u32[]{:S(2)}) copy-start(bf16[2048,64]{0,1:T(8,128)(2,1)} %param.20) | copy-start | bytes 786436
  6.5 32.3 %copy-start.2 = (bf16[1,256,2048]{2,1,0:T(8,128)(2,1)S(1)}, bf16[1,256,2048]{2,1,0:T(8,128)(2,1)}, u32[]{:S(2)}) copy-start(bf16[1,256,2048]{2,1,0:T(8,128)(2,1)} %param.16) | copy-start | bytes 3145732
  6.5 32.3 %copy-start.11 = (f32[2048]{0:T(1024)S(1)}, f32[2048]{0:T(1024)}, u32[]{:S(2)}) copy-start(f32[2048]{0:T(1024)} %param.17) | copy-start | bytes 24580
  6.5 32.3 %all-gather.4.cloned.1.call-start = ((), (), s32[]{:S(2)}) async-start(), calls=%async_computation.2 | async-start | bytes 3538944 | tf_op jit(solution)/shard_map/all_gather | solution.py:20
  8.5 102.3 %all-gather.6.cloned.1.call-start = ((), (), s32[]{:S(2)}) async-start(), calls=%async_computation.3 | async-start | bytes 7798784 | tf_op jit(solution)/shard_map/all_gather | solution.py:20
  41.2 2.1 copy-start.7
  41.3 2.2 %copy-start.8 = (f32[256]{0:T(256)S(1)}, f32[256]{0:T(256)}, u32[]{:S(2)}) copy-start(f32[256]{0:T(256)} %param.22) | copy-start | bytes 3076
  41.3 3.2 %copy-start.3 = (bf16[64,192]{1,0:T(8,128)(2,1)S(1)}, bf16[64,192]{1,0:T(8,128)(2,1)}, u32[]{:S(2)}) copy-start(bf16[64,192]{1,0:T(8,128)(2,1)} %param.23) | copy-start | bytes 73732
  41.3 8.7 %copy-start.5 = (bf16[32,128]{1,0:T(8,128)(2,1)S(1)}, bf16[32,128]{1,0:T(8,128)(2,1)}, u32[]{:S(2)}) copy-start(bf16[32,128]{1,0:T(8,128)(2,1)} %param.24) | copy-start | bytes 24580
  41.3 22.5 %copy-start.6 = (bf16[32,128]{1,0:T(8,128)(2,1)S(1)}, bf16[32,128]{1,0:T(8,128)(2,1)}, u32[]{:S(2)}) copy-start(bf16[32,128]{1,0:T(8,128)(2,1)} %param.25) | copy-start | bytes 24580
  45.2 70.2 %all-to-all-start = ((bf16[8,64,192]{2,1,0:T(8,128)(2,1)}), bf16[8,64,192]{2,1,0:T(8,128)(2,1)}, u32[]{:S(2)}, u32[]{:S(2)}) async-start(bf16[8,64,192]{2,1,0:T(8,128)(2,1)} %broadcast_in_dim.11), calls=%async_computation | async-start | bytes 524288 | tf_op jit(solution)/shard_map/all_to_all | solution.py:31
  49.2 160.5 %all-gather.8.cloned.1.call-start = ((), (), s32[]{:S(2)}) async-start(), calls=%async_computation.4 | async-start | bytes 8454144 | tf_op jit(solution)/shard_map/all_gather | solution.py:165
  115.5 3.8 %copy-start.9 = (f32[192]{0:T(256)S(1)}, f32[192]{0:T(256)}, u32[]{:S(2)}) copy-start(f32[192]{0:T(256)} %param.27) | copy-start | bytes 2308
  119.3 0.7 copy-start.10
  130.0 1.3 copy-start.1
  137.4 1.3 copy-start.1
  144.7 1.3 copy-start.1
  152.0 1.3 copy-start.1
  159.4 1.3 copy-start.1
  166.7 1.3 copy-start.1
  174.0 1.4 copy-start.1
  181.4 1.3 copy-start.1
  207.1 2.2 %copy-start.4 = (f32[2048]{0:T(1024)S(1)}, f32[2048]{0:T(1024)}, u32[]{:S(2)}) copy-start(f32[2048]{0:T(1024)} %param.28) | copy-start | bytes 24580
Sparse Core Ops, SparseCore 0:
  9.0 29.7 all-gather.3
  44.6 66.1 all-gather.5
  113.8 67.8 all-gather.7
where the time goes:
time: 226 us; the launch traced here: 223 us
  waiting for transfers between devices  61.7 us (27%)
  matrix products  60.5 us (27%)
  blocking collectives  46.7 us (21%)
  other arithmetic  22.3 us (10%)
  between operations  13.5 us (6%)
  local copies, waits for them, and re-layouts  8.95 us (4%)
  loops' own time  5.22 us (2%)
  starting transfers between devices  4.13 us (2%)
    all_gather x2, waiting for transfers between devices, in_one_piece(): lax.all_gather(both, axis, axis=dim, tiled=True)  61 us
    dot_general x8, matrix products, one_block(): jnp.einsum('hqk,khd->qhd', weights, value_heads, preferred_element_type=j...  22.6 us
    all_to_all x1, blocking collectives, per_device(): lax.all_to_all(attended, 'sp', split_axis=0, concat_axis=1, tiled=True)  20 us
    dot_general x8, matrix products, one_block(): jnp.einsum('qhd,khd->hqk', query_block, key_heads, preferred_element_type...  15.7 us
    all_gather x1, blocking collectives, per_device(): lax.all_gather(w_key_up, 'dp', axis=0, tiled=True)  13.8 us
    all_gather x1, blocking collectives, per_device(): lax.all_gather(w_value_up, 'dp', axis=0, tiled=True)  12.9 us
    dot_general x2, matrix products, single_fold(): return jnp.dot(inputs, piece, preferred_element_type=jnp.float32)  10.4 us
    reduce_sum x8, other arithmetic, one_block(): weights = jax.nn.softmax(scores, axis=-1).astype(jnp.bfloat16)  10.2 us
  transfers between devices with their start and end apart: 4, of which 2 were waited for; matrix products, arithmetic and copies ran while one was open for 35% of the time, Pallas kernels for 0%

commit v1 on v0

v1 whole, which is shorter than its diff:
```python
import functools

import jax
import jax.numpy as jnp
import numpy as np
from jax import lax
from jax.experimental import pallas as pl
from jax.experimental.pallas import tpu as pltpu
from jax.sharding import PartitionSpec as P

HEADS, NOPE, ROPE, VD, QR, KR, QK = 16, 128, 64, 128, 512, 256, 192
D = 2048
ROWS = 256
EPS = 1e-06
THETA = 10000.0
NEG_BIG = -1e30
BF, F32 = jnp.bfloat16, jnp.float32
SOFT = float(QK**-0.5 * np.log2(np.e))
GROUP = 4


def rope_tables(blocks):
    half = ROPE // 2
    freq = THETA ** (-np.arange(half) / half)
    low = np.arange(ROWS)[:, None] * freq[None, :]
    high = (np.arange(blocks) * ROWS)[:, None] * freq[None, :]
    pad = np.zeros((ROWS, 128 - ROPE))
    lowq = np.stack([np.concatenate([f(low), f(low), pad], 1) for f in (np.cos, np.sin)])
    hpad = np.zeros((blocks, 128 - ROPE))
    highq = np.stack([np.concatenate([f(high), f(high), hpad], 1) for f in (np.cos, np.sin)], 1)
    highq = np.broadcast_to(highq[:, :, None, :], (blocks, 2, 8, 128))
    lowk = np.concatenate([np.cos(low).T, np.sin(low).T], 0)
    highk = np.concatenate([np.cos(high), np.sin(high)], 1)
    highk = np.broadcast_to(highk[:, :, None], (blocks, ROPE, 128))
    return [np.ascontiguousarray(t, dtype=np.float32) for t in (lowq, highq, lowk, highk)]


def dot(a, b):
    return lax.dot_general(a, b, (((1,), (0,)), ((), ())), preferred_element_type=F32)


def dot_nt(a, b):
    return lax.dot_general(a, b, (((1,), (1,)), ((), ())), preferred_element_type=F32)


def prepare_up(u_ref, wq_ref, wkt_ref, wv_ref):
    def one(h, _):
        wq_ref[h] = u_ref[h, :, 0:64, :].reshape(QR, 256)
        kv = u_ref[h, :, 64:96, :].reshape(KR, 256)
        wkt_ref[h] = kv[:, 0:NOPE].T
        wv_ref[h] = kv[:, NOPE:256]
        return 0

    lax.fori_loop(0, HEADS, one, 0)


def make_queries(latq, block, wq_ref, qgain, lowq_ref, highq_ref, q_ref):
    ch, sh = highq_ref[block, 0, 0:1], highq_ref[block, 1, 0:1]
    cl, sl = lowq_ref[0], lowq_ref[1]
    cosine = ch * cl - sh * sl
    sine = sh * cl + ch * sl
    lane = lax.broadcasted_iota(jnp.int32, (ROWS, 128), 1)
    sine_a = jnp.where(lane < ROPE // 2, -sine, 0.0)
    sine_b = jnp.where(lane < ROPE // 2, 0.0, sine)

    def one(h, _):
        q = dot(latq, wq_ref[h])
        scale = lax.rsqrt(jnp.sum(q * q, axis=1, keepdims=True) * (1.0 / QK) + EPS)
        n = q * scale * qgain
        t = n[:, NOPE:256]
        turned = (
            t * cosine
            + pltpu.roll(t, 128 - ROPE // 2, 1) * sine_a
            + pltpu.roll(t, ROPE // 2, 1) * sine_b
        )
        q_ref[h, :, 0:NOPE] = n[:, 0:NOPE].astype(BF)
        q_ref[h, :, NOPE:256] = turned.astype(BF)
        return 0

    lax.fori_loop(0, HEADS, one, 0)


def expand(unit, block, wkt_ref, wv_ref, gk_ref, gr_ref, lowk_ref, highk_ref, kt_ref, v_ref):
    kv = unit[0:256, :]
    rope = unit[256:320, :].astype(F32)
    half = ROPE // 2
    ch = jnp.concatenate([highk_ref[block, 0:half]] * 2, axis=1)
    sh = jnp.concatenate([highk_ref[block, half:ROPE]] * 2, axis=1)
    cl, sl = lowk_ref[0:half], lowk_ref[half:ROPE]
    cosine = ch * cl - sh * sl
    sine = sh * cl + ch * sl
    rope_sq = jnp.sum(rope * rope, axis=0, keepdims=True)
    x = rope * gr_ref[...]
    a, b = x[0:half], x[half:ROPE]
    turned = jnp.concatenate([a * cosine - b * sine, b * cosine + a * sine], axis=0)

    def one(g, _):
        heads = pl.ds(g * GROUP, GROUP)
        kt = dot_nt(wkt_ref[heads].reshape(GROUP * NOPE, KR), kv)
        for i in range(GROUP):
            k = kt[i * NOPE : (i + 1) * NOPE]
            scale = lax.rsqrt(
                (jnp.sum(k * k, axis=0, keepdims=True) + rope_sq) * (1.0 / QK) + EPS
            )
            kt_ref[g * GROUP + i, 0:NOPE] = (k * scale * gk_ref[...]).astype(BF)
            kt_ref[g * GROUP + i, NOPE:QK] = (turned * scale).astype(BF)
            v_ref[g * GROUP + i, :, 0:VD] = dot(kv, wv_ref[g * GROUP + i]).astype(BF)
        return 0

    lax.fori_loop(0, HEADS // GROUP, one, 0)


def attend(diagonal, q_ref, kt_ref, v_ref, m_ref, acc_ref):
    def one(g, _):
        for i in range(GROUP):
            h = g * GROUP + i
            s = dot(q_ref[h], kt_ref[h])
            if diagonal:
                row = lax.broadcasted_iota(jnp.int32, (ROWS, ROWS), 0)
                col = lax.broadcasted_iota(jnp.int32, (ROWS, ROWS), 1)
                s = jnp.where(col <= row, s, NEG_BIG)
            top = jnp.max(s, axis=1, keepdims=True)
            if diagonal:
                p = jnp.exp2((s - top) * SOFT).astype(BF)
                m_ref[h] = jnp.broadcast_to(top, (ROWS, 128))
                acc_ref[h] = dot(p, v_ref[h])
            else:
                old = m_ref[h]
                new = jnp.maximum(old, top)
                fade = jnp.exp2((old - new) * SOFT)
                p = jnp.exp2((s - jnp.concatenate([new, new], 1)) * SOFT).astype(BF)
                m_ref[h] = new
                acc_ref[h] = acc_ref[h] * jnp.concatenate([fade, fade], 1) + dot(p, v_ref[h])
        return 0

    lax.fori_loop(0, HEADS // GROUP, one, 0)


def finish(acc_ref, mixed_ref, ogain_ref, wout_ref, out_ref):
    total = jnp.zeros((ROWS, VD), F32)
    for h in range(HEADS):
        at = (acc_ref[h, :, 0:VD] / acc_ref[h, :, VD : 2 * VD]).astype(BF)
        mixed_ref[:, h * VD : (h + 1) * VD] = at
        total = total + at.astype(F32) * at.astype(F32)
    scale = lax.rsqrt(jnp.sum(total, axis=1, keepdims=True) * (1.0 / (HEADS * VD)) + EPS)
    for h in range(HEADS):
        cols = slice(h * VD, (h + 1) * VD)
        mixed_ref[:, cols] = (mixed_ref[:, cols].astype(F32) * scale * ogain_ref[:, cols]).astype(BF)

    def one(j, _):
        cols = pl.ds(pl.multiple_of(j * 256, 256), 256)
        out_ref[:, cols] = dot(mixed_ref[...], wout_ref[:, cols]).astype(BF)
        return 0

    lax.fori_loop(0, D // 256, one, 0)


def main_kernel(
    latq_ref, kv_ref, u_ref, wout_hbm, qgain_ref, gk_ref, gr_ref, ogain_ref,
    lowq_ref, highq_ref, lowk_ref, highk_ref, out_ref,
    wq_ref, wkt_ref, wv_ref, q_ref, kt_ref, v_ref, m_ref, acc_ref, mixed_ref, wout_ref, sem,
):
    me = lax.axis_index("sp")
    load = pltpu.make_async_copy(wout_hbm, wout_ref, sem)
    load.start()
    prepare_up(u_ref, wq_ref, wkt_ref, wv_ref)
    make_queries(latq_ref[...], me, wq_ref, qgain_ref[...], lowq_ref, highq_ref, q_ref)
    kt_ref[:, QK:256, :] = jnp.zeros((HEADS, 256 - QK, 256), BF)
    v_ref[:, :, VD:256] = jnp.ones((HEADS, ROWS, 256 - VD), BF)

    def block(b):
        expand(
            kv_ref[b], b, wkt_ref, wv_ref, gk_ref, gr_ref, lowk_ref, highk_ref, kt_ref, v_ref
        )

    block(me)
    attend(True, q_ref, kt_ref, v_ref, m_ref, acc_ref)

    def one(i, _):
        block(i)
        attend(False, q_ref, kt_ref, v_ref, m_ref, acc_ref)
        return 0

    lax.fori_loop(0, me, one, 0)
    load.wait()
    finish(acc_ref, mixed_ref, ogain_ref, wout_ref, out_ref)


def rms_scale(values, scaling):
    return values * lax.rsqrt(jnp.mean(values * values, axis=-1, keepdims=True) + EPS) * scaling


def per_device(
    tokens, in_gain, w_query_down, w_latent_down, w_rope_key, query_latent_gain, latent_gain,
    w_query_up, w_key_up, w_value_up, query_gain, key_gain, out_gain, w_out,
):
    blocks = lax.axis_size("sp")
    wout = lax.all_gather(w_out, ("sp", "dp"), axis=0, tiled=True)
    up = jnp.concatenate(
        [
            jnp.pad(w_query_up, ((0, 0), (0, 256 - QK))),
            jnp.concatenate([w_key_up, w_value_up], axis=1),
        ],
        axis=0,
    )
    down = lax.all_gather(
        jnp.concatenate([w_query_down, w_latent_down], axis=1), "dp", axis=0, tiled=True
    )
    ups = lax.all_gather(up, ("sp", "dp"), axis=0, tiled=True).reshape(HEADS, 8, 96, 256)
    rows = tokens.reshape(ROWS, D)
    normed = rms_scale(rows.astype(F32), in_gain).astype(BF)
    both = dot(normed, down)
    latent_q = rms_scale(both[:, :QR], query_latent_gain).astype(BF)
    latent_kv = rms_scale(both[:, QR:], latent_gain).astype(BF)
    rope_t = dot_nt(w_rope_key.T, normed).astype(BF)
    unit = jnp.concatenate([latent_kv, rope_t], axis=0)
    units = lax.all_gather(unit, "sp", axis=0, tiled=True).reshape(blocks, 320, 256)
    tables = [jnp.asarray(t) for t in rope_tables(blocks)]
    qgain = jnp.pad(query_gain, (0, 256 - QK)).reshape(1, 256)
    gk = jnp.broadcast_to(key_gain[:NOPE, None], (NOPE, 256))
    gr = jnp.broadcast_to(key_gain[NOPE:, None], (ROPE, 256))
    vm = pl.BlockSpec(memory_space=pltpu.VMEM)
    out = pl.pallas_call(
        main_kernel,
        out_shape=jax.ShapeDtypeStruct((ROWS, D), BF),
        in_specs=[vm, vm, vm, pl.BlockSpec(memory_space=pl.ANY)] + [vm] * 8,
        out_specs=vm,
        scratch_shapes=[
            pltpu.VMEM((HEADS, QR, 256), BF),
            pltpu.VMEM((HEADS, NOPE, KR), BF),
            pltpu.VMEM((HEADS, KR, VD), BF),
            pltpu.VMEM((HEADS, ROWS, 256), BF),
            pltpu.VMEM((HEADS, 256, 256), BF),
            pltpu.VMEM((HEADS, 256, 256), BF),
            pltpu.VMEM((HEADS, ROWS, 128), F32),
            pltpu.VMEM((HEADS, ROWS, 256), F32),
            pltpu.VMEM((ROWS, D), BF),
            pltpu.VMEM((D, D), BF),
            pltpu.SemaphoreType.DMA,
        ],
        compiler_params=pltpu.CompilerParams(vmem_limit_bytes=58 * 1024 * 1024),
        cost_estimate=pl.CostEstimate(flops=20_000_000_000, bytes_accessed=20_000_000, transcendentals=0),
    )(latent_q, units, ups, wout, qgain, gk, gr, out_gain.reshape(1, D), *tables)
    return out.reshape(1, ROWS, D)


def solution(mesh):
    in_specs = (
        P("dp", "sp", None), P(), P("dp", None), P("dp", None), P(), P(), P(),
        P("dp", "sp"), P("dp", "sp"), P("dp", "sp"), P(), P(), P(), P(("sp", "dp"), None),
    )
    return jax.shard_map(
        per_device, mesh=mesh, in_specs=in_specs, out_specs=P("dp", "sp", None), check_vma=False
    )
```

time: 226 us -> 317 us (1.40)
  the two profiles are of different devices: /device:TPU:24 before, /device:TPU:121 now
where the time goes in v1:
time: 317 us
  waiting for transfers between devices  210 us (66%)
  Pallas kernels  82.7 us (26%)
  between operations  13.3 us (4%)
  other arithmetic  5.88 us (2%)
  matrix products  3.42 us (1%)
    pallas_call x1, Pallas kernels, per_device(): pl.pallas_call(main_kernel, out_shape=jax.ShapeDtypeStruct((ROWS, D), BF)...  82.7 us
    all_gather x1, waiting for transfers between devices, per_device(): lax.all_gather(up, ('sp', 'dp'), axis=0, tiled=True)  71.8 us
    all_gather x1, waiting for transfers between devices, per_device(): wout = lax.all_gather(w_out, ('sp', 'dp'), axis=0, tiled=True)  70 us
    all_gather x1, waiting for transfers between devices, per_device(): lax.all_gather(unit, 'sp', axis=0, tiled=True).reshape(blocks, 320, 256)  39.7 us
    all_gather x1, waiting for transfers between devices, per_device(): lax.all_gather(jnp.concatenate([w_query_down, w_latent_down], axis=1), 'd...  27.5 us
  transfers between devices with their start and end apart: 4, of which 4 were waited for; matrix products, arithmetic and copies ran while one was open for 1% of the time, Pallas kernels for 0%

profile of v1, /device:TPU:121, one launch (start us, length us, event | category | flops | bytes accessed | tf_op | source)
XLA Modules:
  0.0 317.1 jit_solution(7825979925810480220)
XLA Ops:
  6.5 0.0 copy-start
  6.5 0.0 copy-start.1
  6.5 0.0 copy-start.9
  6.5 0.0 all-gather.5.cloned.1.call-start
  6.5 1.9 pad_maximum_fusion
  8.4 0.0 all-gather.5.cloned.1.call-update
  8.5 0.0 all-gather.7.cloned.1.call-start
  8.5 1.5 fusion
  10.0 0.0 copy-done
  10.0 0.0 copy-done.1
  10.1 0.0 copy-done.9
  10.1 0.5 fusion.3
  10.6 0.0 copy-start.6
  10.6 0.0 copy-start.2
  10.6 0.0 copy-start.3
  10.6 0.0 copy-start.4
  10.6 0.0 copy-start.8
  10.6 0.0 copy-start.7
  10.6 0.0 copy-start.5
  10.7 27.5 %all-gather.5.cloned.1.call-done = bf16[2048,768]{1,0:T(8,128)(2,1)} async-done(((bf16[256,768]{1,0:T(8,128)(2,1)}), bf16[2048,768]{1,0:T(8,128)(2,1)}) %all-gather.5.cloned.1.call-update) | async-done | bytes 3145744 | tf_op jit(solution)/shard_map/all_gather | solution.py:206
  38.1 2.9 fusion.5
  41.1 0.0 slice-start
  41.1 0.1 multiply_reduce_fusion.1
  41.2 0.0 copy-done.6
  41.2 0.1 multiply_convert_fusion.1
  41.3 0.7 pad_maximum_fusion.1
  42.0 0.0 all-gather.7.cloned.1.call-update
  42.0 0.0 all-gather.9.cloned.1.call-start
  42.1 0.0 copy-done.2
  42.1 0.0 copy-done.3
  42.1 0.0 copy-done.4
  42.1 0.6 fusion.8
  42.7 0.0 all-gather.9.cloned.1.call-update
  42.8 0.0 all-gather.11.cloned.1.call-start
  42.8 0.5 all-gather.11.cloned.1.call-update
  43.3 0.0 copy-done.8
  43.4 0.0 copy-done.7
  43.4 0.6 pad.9
  44.0 0.1 multiply_reduce_fusion
  44.1 0.0 copy-done.5
  44.1 0.8 multiply_convert_fusion.latq_ref
  44.9 39.7 %all-gather.7.cloned.1.call-done = bf16[5120,256]{1,0:T(8,128)(2,1)} async-done(((bf16[320,256]{1,0:T(8,128)(2,1)}), bf16[5120,256]{1,0:T(8,128)(2,1)}) %all-gather.7.cloned.1.call-update) | async-done | bytes 2621456 | tf_op jit(solution)/shard_map/all_gather | solution.py:217
  84.6 71.8 %all-gather.9.cloned.1.call-done = bf16[12288,256]{1,0:T(8,128)(2,1)} async-done(((bf16[96,256]{1,0:T(8,128)(2,1)}), bf16[12288,256]{1,0:T(8,128)(2,1)}) %all-gather.9.cloned.1.call-update) | async-done | bytes 6291472 | tf_op jit(solution)/shard_map/all_gather | solution.py:209
  156.4 70.0 %all-gather.11.cloned.1.call-done.wout_hbm = bf16[2048,2048]{1,0:T(8,128)(2,1)} async-done(((bf16[16,2048]{1,0:T(8,128)(2,1)}), bf16[2048,2048]{1,0:T(8,128)(2,1)}) %all-gather.11.cloned.1.call-update) | async-done | bytes 8388624 | tf_op jit(solution)/shard_map/all_gather | solution.py:198
  226.4 0.0 slice-done
  226.4 0.7 broadcast_in_dim.4.gk_ref
  227.2 0.7 broadcast_in_dim.5.gr_ref
  227.8 82.7 %shard_map.172 = bf16[256,2048]{1,0:T(8,128)(2,1)} custom-call(bf16[256,512]{1,0:T(8,128)(2,1)} %multiply_convert_fusion.latq_ref, bf16[16,320,256]{2,1,0:T(8,128)(2,1)} %bitcast.17, bf16[16,8,96,256]{3,2,1,0:T(8,128)(2,1)} %bitcast.16, bf16[2048,2048]{1,0:T(8,128)(2,1)} %all-gather.11.cloned.1.call-done.wout_hbm, f32[1,256]{1,0:T(1,128)} %bitcast.15, ...), custom_call_target="tpu_custom_call" | custom-call | flops 20000000000 | bytes 20000000 | tf_op jit(solution)/shard_map/pallas_call | solution.py:223
  (4 shorter events, 0.0 us)
Async XLA Ops:
  6.5 3.5 %copy-start = (bf16[2048,64]{0,1:T(8,128)(2,1)S(1)}, bf16[2048,64]{0,1:T(8,128)(2,1)}, u32[]{:S(2)}) copy-start(bf16[2048,64]{0,1:T(8,128)(2,1)} %param.22) | copy-start | bytes 786436
  6.5 3.5 %copy-start.1 = (bf16[1,256,2048]{2,1,0:T(8,128)(2,1)S(1)}, bf16[1,256,2048]{2,1,0:T(8,128)(2,1)}, u32[]{:S(2)}) copy-start(bf16[1,256,2048]{2,1,0:T(8,128)(2,1)} %param.18) | copy-start | bytes 3145732
  6.5 3.5 %copy-start.9 = (f32[2048]{0:T(1024)S(1)}, f32[2048]{0:T(1024)}, u32[]{:S(2)}) copy-start(f32[2048]{0:T(1024)} %param.19) | copy-start | bytes 24580
  6.5 31.6 %all-gather.5.cloned.1.call-start = ((), (), s32[]{:S(2)}) async-start(), calls=%async_computation | async-start | bytes 3538944 | tf_op jit(solution)/shard_map/all_gather | solution.py:206
  8.5 76.1 %all-gather.7.cloned.1.call-start = ((), (), s32[]{:S(2)}) async-start(), calls=%async_computation.1 | async-start | bytes 2785280 | tf_op jit(solution)/shard_map/all_gather | solution.py:217
  10.6 30.6 %copy-start.6 = (f32[256]{0:T(256)S(1)}, f32[256]{0:T(256)}, u32[]{:S(2)}) copy-start(f32[256]{0:T(256)} %param.24) | copy-start | bytes 3076
  10.6 31.5 %copy-start.2 = (bf16[64,192]{1,0:T(8,128)(2,1)S(1)}, bf16[64,192]{1,0:T(8,128)(2,1)}, u32[]{:S(2)}) copy-start(bf16[64,192]{1,0:T(8,128)(2,1)} %param.25) | copy-start | bytes 73732
  10.6 31.5 %copy-start.3 = (bf16[32,128]{1,0:T(8,128)(2,1)S(1)}, bf16[32,128]{1,0:T(8,128)(2,1)}, u32[]{:S(2)}) copy-start(bf16[32,128]{1,0:T(8,128)(2,1)} %param.27) | copy-start | bytes 24580
  10.6 31.5 %copy-start.4 = (bf16[32,128]{1,0:T(8,128)(2,1)S(1)}, bf16[32,128]{1,0:T(8,128)(2,1)}, u32[]{:S(2)}) copy-start(bf16[32,128]{1,0:T(8,128)(2,1)} %param.26) | copy-start | bytes 24580
  10.6 32.7 %copy-start.8 = (f32[192]{0:T(256)S(1)}, f32[192]{0:T(256)}, u32[]{:S(2)}) copy-start(f32[192]{0:T(256)} %param.29) | copy-start | bytes 2308
  10.6 32.7 %copy-start.7 = (f32[192]{0:T(256)S(1)}, f32[192]{0:T(256)}, u32[]{:S(2)}) copy-start(f32[192]{0:T(256)} %param.28) | copy-start | bytes 2308
  10.6 33.4 %copy-start.5 = (f32[512]{0:T(512)S(1)}, f32[512]{0:T(512)}, u32[]{:S(2)}) copy-start(f32[512]{0:T(512)} %param.23) | copy-start | bytes 6148
  41.1 185.4 %slice-start = ((f32[192]{0:T(256)}), f32[128]{0:T(128)S(1)}, s32[]{:S(2)}) async-start(f32[192]{0:T(256)} %param.29), calls=%async_computation.4 | async-start | bytes 1024 | tf_op jit(solution)/shard_map/slice | solution.py:220
  42.0 114.4 %all-gather.9.cloned.1.call-start = ((), (), s32[]{:S(2)}) async-start(), calls=%async_computation.2 | async-start | bytes 6340608 | tf_op jit(solution)/shard_map/all_gather | solution.py:209
  42.8 183.7 %all-gather.11.cloned.1.call-start = ((), (), s32[]{:S(2)}) async-start(), calls=%async_computation.3 | async-start | bytes 8454144 | tf_op jit(solution)/shard_map/all_gather | solution.py:198
Sparse Core Ops, SparseCore 0:
  9.0 29.0 all-gather.4
  42.1 42.3 all-gather.6
  87.7 68.6 all-gather.8
  159.2 67.1 all-gather.10

commit v2 on v1

v2 whole, which is shorter than its diff:
```python
import functools

import jax
import jax.numpy as jnp
import numpy as np
from jax import lax
from jax.experimental import pallas as pl
from jax.experimental.pallas import tpu as pltpu
from jax.sharding import PartitionSpec as P

HEADS, NOPE, ROPE, VD, QR, KR, QK = 16, 128, 64, 128, 512, 256, 192
D = 2048
ROWS = 256
EPS = 1e-06
THETA = 10000.0
NEG_BIG = -1e30
BF, F32 = jnp.bfloat16, jnp.float32
SOFT = float(QK**-0.5 * np.log2(np.e))
LOCAL = 8


def rope_tables(blocks):
    half = ROPE // 2
    freq = THETA ** (-np.arange(half) / half)
    low = np.arange(ROWS)[:, None] * freq[None, :]
    high = (np.arange(blocks) * ROWS)[:, None] * freq[None, :]
    pad = np.zeros((ROWS, 128 - ROPE))
    lowq = np.stack([np.concatenate([f(low), f(low), pad], 1) for f in (np.cos, np.sin)])
    hpad = np.zeros((blocks, 128 - ROPE))
    highq = np.stack([np.concatenate([f(high), f(high), hpad], 1) for f in (np.cos, np.sin)], 1)
    highq = np.broadcast_to(highq[:, :, None, :], (blocks, 2, 8, 128))
    lowk = np.concatenate([np.cos(low).T, np.sin(low).T], 0)
    highk = np.concatenate([np.cos(high), np.sin(high)], 1)
    highk = np.broadcast_to(highk[:, :, None], (blocks, ROPE, 128))
    return [np.ascontiguousarray(t, dtype=np.float32) for t in (lowq, highq, lowk, highk)]


def dot(a, b):
    return lax.dot_general(a, b, (((1,), (0,)), ((), ())), preferred_element_type=F32)


def dot_nt(a, b):
    return lax.dot_general(a, b, (((1,), (1,)), ((), ())), preferred_element_type=F32)


def prepare_up(us, wq_ref, wkt_ref, wv_ref):
    def one(h, _):
        for x in range(4):
            for c in range(2):
                d = 2 * x + c
                unit = us[c, h, x]
                wq_ref[h, d * 64 : d * 64 + 64] = unit[0:64]
                kv_rows = slice(d * 32, d * 32 + 32)
                wv_ref[h, kv_rows] = unit[64:96, NOPE:256]
                wkt_ref[h, kv_rows] = unit[64:96, 0:NOPE]
        return 0

    lax.fori_loop(0, LOCAL, one, 0)


def transpose_keys(wk_ref, wkt_ref):
    def one(h, _):
        wkt_ref[h] = wk_ref[h].T
        return 0

    lax.fori_loop(0, LOCAL, one, 0)


def make_queries(latq, block, wq_ref, qgain, lowq_ref, highq_ref, q_ref, which):
    ch, sh = highq_ref[block, 0, 0:1], highq_ref[block, 1, 0:1]
    cl, sl = lowq_ref[0], lowq_ref[1]
    cosine = ch * cl - sh * sl
    sine = sh * cl + ch * sl
    lane = lax.broadcasted_iota(jnp.int32, (ROWS, 128), 1)
    sine_a = jnp.where(lane < ROPE // 2, -sine, 0.0)
    sine_b = jnp.where(lane < ROPE // 2, 0.0, sine)

    def one(g, _):
        for i in range(2):
            h = g * 2 + i
            q = dot(latq, wq_ref[h])
            scale = lax.rsqrt(jnp.sum(q * q, axis=1, keepdims=True) * (1.0 / QK) + EPS)
            n = q * scale * qgain
            t = n[:, NOPE:256]
            turned = (
                t * cosine
                + pltpu.roll(t, 128 - ROPE // 2, 1) * sine_a
                + pltpu.roll(t, ROPE // 2, 1) * sine_b
            )
            q_ref[which, h, :, 0:NOPE] = n[:, 0:NOPE].astype(BF)
            q_ref[which, h, :, NOPE:256] = turned.astype(BF)
        return 0

    lax.fori_loop(0, LOCAL // 2, one, 0)


def expand(unit, block, wkt_ref, wv_ref, gk_ref, gr_ref, lowk_ref, highk_ref, kt_ref, v_ref, slot):
    kv = unit[0:256, :]
    rope = unit[256:320, :].astype(F32)
    half = ROPE // 2
    ch = jnp.concatenate([highk_ref[block, 0:half]] * 2, axis=1)
    sh = jnp.concatenate([highk_ref[block, half:ROPE]] * 2, axis=1)
    cl, sl = lowk_ref[0:half], lowk_ref[half:ROPE]
    cosine = ch * cl - sh * sl
    sine = sh * cl + ch * sl
    rope_sq = jnp.sum(rope * rope, axis=0, keepdims=True)
    x = rope * gr_ref[...]
    a, b = x[0:half], x[half:ROPE]
    turned = jnp.concatenate([a * cosine - b * sine, b * cosine + a * sine], axis=0)
    kt = dot_nt(wkt_ref[...].reshape(LOCAL * NOPE, KR), kv)
    for h in range(LOCAL):
        k = kt[h * NOPE : (h + 1) * NOPE]
        scale = lax.rsqrt((jnp.sum(k * k, axis=0, keepdims=True) + rope_sq) * (1.0 / QK) + EPS)
        kt_ref[slot, h, 0:NOPE] = (k * scale * gk_ref[...]).astype(BF)
        kt_ref[slot, h, NOPE:QK] = (turned * scale).astype(BF)
    for h in range(LOCAL):
        v_ref[slot, h, :, 0:VD] = dot(kv, wv_ref[h]).astype(BF)


def attend(diagonal, q_ref, kt_ref, v_ref, m_ref, acc_ref, which, slot):
    for h in range(LOCAL):
        s = dot(q_ref[which, h], kt_ref[slot, h])
        if diagonal:
            row = lax.broadcasted_iota(jnp.int32, (ROWS, ROWS), 0)
            col = lax.broadcasted_iota(jnp.int32, (ROWS, ROWS), 1)
            s = jnp.where(col <= row, s, NEG_BIG)
        old = m_ref[which, h]
        new = jnp.maximum(old, jnp.max(s, axis=1, keepdims=True))
        fade = jnp.exp2((old - new) * SOFT)
        p = jnp.exp2((s - jnp.concatenate([new, new], 1)) * SOFT).astype(BF)
        m_ref[which, h] = new
        acc_ref[which, h] = acc_ref[which, h] * jnp.concatenate([fade, fade], 1) + dot(
            p, v_ref[slot, h]
        )


def close_heads(acc_ref, which, att_ref, first):
    for h in range(LOCAL):
        att_ref[first + h] = (
            acc_ref[which, h, :, 0:VD] / acc_ref[which, h, :, VD : 2 * VD]
        ).astype(BF)


def finish(att_ref, mixed_ref, ogain_ref, wo_ref, out_ref):
    total = jnp.zeros((ROWS, VD), F32)
    for h in range(HEADS):
        at = att_ref[h].astype(F32)
        total = total + at * at
    scale = lax.rsqrt(jnp.sum(total, axis=1, keepdims=True) * (1.0 / (HEADS * VD)) + EPS)
    for h in range(HEADS):
        cols = slice(h * VD, (h + 1) * VD)
        mixed_ref[:, cols] = (att_ref[h].astype(F32) * scale * ogain_ref[:, cols]).astype(BF)

    def one(j, _):
        cols = pl.ds(pl.multiple_of(j * 256, 256), 256)
        w = wo_ref[:, :, :, :, :, cols].reshape(HEADS * VD, 256)
        out_ref[:, cols] = dot(mixed_ref[...], w).astype(BF)
        return 0

    lax.fori_loop(0, D // 256, one, 0)


def rms_rows(values, scaling):
    return values * lax.rsqrt(jnp.mean(values * values, axis=-1, keepdims=True) + EPS) * scaling


SLOTS = 128
OPS = 51


def kernel(
    tok_ref, ing_ref, wqd_ref, wld_ref, wrt_ref, qlg_ref, klg_ref, wqu_ref, wku_ref, wvu_ref,
    qgain_ref, gk_ref, gr_ref, ogain_ref, wo_in_ref, lowq_ref, highq_ref, lowk_ref, highk_ref,
    out_ref,
    wd, us, wo, kvb, lq, normed, sums, wq_ref, wk_ref, wkt_ref, wv_ref, q_ref, kt_ref, v_ref,
    m_ref, acc_ref, att_ref, mixed_ref, ssem, rsem,
):
    sp, dp = lax.axis_index("sp"), lax.axis_index("dp")
    z, y = sp // 4, sp % 4
    x, c = dp // 2, dp % 2
    xl, xr, xo = (x + 3) % 4, (x + 1) % 4, (x + 2) % 4
    yl, yr, yo = (y + 3) % 4, (y + 1) % 4, (y + 2) % 4
    zl, zr, zo = (z + 3) % 4, (z + 1) % 4, (z + 2) % 4
    co = 1 - c
    zb = z % 2
    zpair = z + 1 - 2 * zb
    zmate = 3 - z

    def dev(xx=x, yy=y, zz=z, cc=c):
        return {"sp": zz * 4 + yy, "dp": xx * 2 + cc}

    X_R, X_L, Y_R, Y_L, Z_R, Z_L, CORE = (
        dev(xx=xr), dev(xx=xl), dev(yy=yr), dev(yy=yl), dev(zz=zr), dev(zz=zl), dev(cc=co)
    )
    names, sent = {}, []

    def number(name):
        return names.setdefault(name, len(names))

    def push(name, view, to, dst=None):
        i = number(name)
        again = view if callable(view) else functools.partial(lambda v: v, view)
        view = again()
        pltpu.make_async_remote_copy(
            src_ref=view, dst_ref=view if dst is None else dst, send_sem=ssem.at[i],
            recv_sem=rsem.at[i], device_id=to, device_id_type=pl.DeviceIdType.MESH,
        ).start()
        sent.append((i, again))

    def got(name, view):
        pltpu.make_async_copy(view, view, rsem.at[number(name)]).wait()

    barrier = pltpu.get_barrier_semaphore()
    for to in (X_R, X_L, Y_R, Y_L, Z_R, Z_L, CORE):
        pl.semaphore_signal(barrier, 1, device_id=to, device_id_type=pl.DeviceIdType.MESH)

    hl = zb * 4 + y
    us[c, hl, x, 0:64, 0:NOPE] = wqu_ref[:, 0:NOPE]
    us[c, hl, x, 0:64, NOPE:256] = jnp.concatenate(
        [wqu_ref[:, NOPE:QK], jnp.zeros((64, 256 - QK), BF)], axis=1
    )
    us[c, hl, x, 64:96, 0:NOPE] = wku_ref[...]
    us[c, hl, x, 64:96, NOPE:256] = wvu_ref[...]
    wo[z, y, x, c] = wo_in_ref[...]
    wd[dp, :, 0:QR] = wqd_ref[...]
    wd[dp, :, QR : QR + KR] = wld_ref[...]
    pl.semaphore_wait(barrier, 7)

    uown = us.at[c, hl, x]
    push("u_r", uown, X_R)
    push("u_l", uown, X_L)
    wown = wo.at[z, y, x, c]
    push("w_yr", wown, Y_R)
    push("w_yl", wown, Y_L)
    down = wd.at[dp]
    push("d_r", down, X_R)
    push("d_l", down, X_L)
    push("d_c", down, CORE)

    for r in range(0, ROWS, 64):
        rows = slice(r, r + 64)
        n = rms_rows(tok_ref[rows].astype(F32), ing_ref[...]).astype(BF)
        for k in range(8):
            normed[k, rows] = n[:, k * 256 : (k + 1) * 256]

    got("u_r", us.at[c, hl, xl])
    push("u_or", us.at[c, hl, xl, 0:48], X_R)
    got("u_l", us.at[c, hl, xr])
    push("u_ol", us.at[c, hl, xr, 48:96], X_L)
    got("w_yr", wo.at[z, yl, x, c])
    push("w_oyr", wo.at[z, yl, x, c, :, 0:1024], Y_R)
    got("w_yl", wo.at[z, yr, x, c])
    push("w_oyl", wo.at[z, yr, x, c, :, 1024:2048], Y_L)
    got("u_or", us.at[c, hl, xo, 0:48])
    got("u_ol", us.at[c, hl, xo, 48:96])
    block0 = us.at[c, hl]
    push("u_z", block0, dev(zz=zpair))
    push("u_y0r", block0, Y_R)
    push("u_y0l", block0, Y_L)
    push("u_c0", block0, CORE)
    got("w_oyr", wo.at[z, yo, x, c, :, 0:1024])
    got("w_oyl", wo.at[z, yo, x, c, :, 1024:2048])
    push("w_zr", wo.at[z, :, x, c], Z_R)
    push("w_zl", wo.at[z, :, x, c], Z_L)

    def add(d, first=False):
        part = dot(normed[d], wd[d])
        if first:
            sums[...] = part
        else:
            sums[...] += part

    add(dp, True)
    got("d_c", wd.at[2 * x + co])
    add(2 * x + co)
    base0, base1 = zb * 4, 4 - zb * 4
    got("u_z", us.at[c, base1 + y])
    block1 = us.at[c, base1 + y]
    push("u_c1", block1, CORE)

    def ring_y(j, base):
        got(f"u_y{j}r", us.at[c, base + yl])
        push(f"u_y{j}or", us.at[c, base + yl, 0:2], Y_R)
        push(f"u_c{j}l", us.at[c, base + yl], CORE)
        got(f"u_y{j}l", us.at[c, base + yr])
        push(f"u_y{j}ol", us.at[c, base + yr, 2:4], Y_L)
        push(f"u_c{j}r", us.at[c, base + yr], CORE)

    ring_y(0, base0)
    push("u_y1r", block1, Y_R)
    push("u_y1l", block1, Y_L)
    got("d_r", wd.at[2 * xl + c])
    push("d_or", wd.at[2 * xl + c, 0:128], X_R)
    push("d_cl", wd.at[2 * xl + c], CORE)
    got("d_l", wd.at[2 * xr + c])
    push("d_ol", wd.at[2 * xr + c, 128:256], X_L)
    push("d_cr", wd.at[2 * xr + c], CORE)
    add(2 * xl + c)
    add(2 * xr + c)
    got("d_cl", wd.at[2 * xl + co])
    add(2 * xl + co)
    got("d_cr", wd.at[2 * xr + co])
    add(2 * xr + co)
    got("w_zr", wo.at[zl, :, x, c])
    push("w_ozr", wo.at[zl, 0:2, x, c], Z_R)
    got("w_zl", wo.at[zr, :, x, c])
    push("w_ozl", wo.at[zr, 2:4, x, c], Z_L)
    ring_y(1, base1)
    got("d_or", wd.at[2 * xo + c, 0:128])
    push("d_coa", wd.at[2 * xo + c, 0:128], CORE)
    got("d_ol", wd.at[2 * xo + c, 128:256])
    push("d_cob", wd.at[2 * xo + c, 128:256], CORE)
    rope_t = jnp.zeros((ROPE, ROWS), F32)
    for k in range(8):
        rope_t = rope_t + dot_nt(wrt_ref[:, k * 256 : (k + 1) * 256], normed[k])
    add(2 * xo + c)
    got("d_coa", wd.at[2 * xo + co, 0:128])
    got("d_cob", wd.at[2 * xo + co, 128:256])
    add(2 * xo + co)

    kvb[y, z, 0:256] = rms_rows(sums[:, QR : QR + KR], klg_ref[...]).astype(BF)
    kvb[y, z, 256:320] = rope_t.astype(BF)
    lq[0] = rms_rows(sums[:, 0:QR], qlg_ref[...]).astype(BF)
    own = kvb.at[y, z]
    push("k_yr", own, Y_R)
    push("k_yl", own, Y_L)
    push("k_zr", own, Z_R)
    push("k_zl", own, Z_L)
    push("q", lq.at[0], dev(zz=zmate), lq.at[1])

    for j, base in ((0, base0), (1, base1)):
        got(f"u_y{j}or", us.at[c, base + yo, 0:2])
        got(f"u_y{j}ol", us.at[c, base + yo, 2:4])
        push(f"u_c{j}o", us.at[c, base + yo], CORE)
    got("w_ozr", wo.at[zo, 0:2, x, c])
    got("w_ozl", wo.at[zo, 2:4, x, c])
    for p in range(2):
        push(f"w_xr{p}", wo.at[2 * p : 2 * p + 2, :, x, c], X_R)
        push(f"w_xl{p}", wo.at[2 * p : 2 * p + 2, :, x, c], X_L)
    for j, base in ((0, base0), (1, base1)):
        got(f"u_c{j}", us.at[co, base + y])
        got(f"u_c{j}l", us.at[co, base + yl])
        got(f"u_c{j}r", us.at[co, base + yr])
        got(f"u_c{j}o", us.at[co, base + yo])
    push("w_c", wo.at[:, :, x, c], CORE)
    prepare_up(us, wq_ref, wk_ref, wv_ref)
    transpose_keys(wk_ref, wkt_ref)
    make_queries(lq[0], sp, wq_ref, qgain_ref[...], lowq_ref, highq_ref, q_ref, 0)
    m_ref[...] = jnp.full(m_ref.shape, NEG_BIG, F32)
    acc_ref[...] = jnp.zeros(acc_ref.shape, F32)
    kt_ref[:, :, QK:256, :] = jnp.zeros((4, LOCAL, 256 - QK, 256), BF)
    v_ref[:, :, :, VD:256] = jnp.ones((4, LOCAL, ROWS, 256 - VD), BF)

    def k1():
        got("k_yr", kvb.at[yl, z])
        push("k_oyr", lambda: kvb.at[yl, z, 0:160], Y_R)
        got("k_yl", kvb.at[yr, z])
        push("k_oyl", lambda: kvb.at[yr, z, 160:320], Y_L)

    def k2():
        got("k_zr", kvb.at[y, zl])
        push("k_ozr", lambda: kvb.at[y, zl, 0:160], Z_R)
        push("k_y1r", lambda: kvb.at[y, zl], Y_R)
        push("k_y1l", lambda: kvb.at[y, zl], Y_L)
        got("k_zl", kvb.at[y, zr])
        push("k_ozl", lambda: kvb.at[y, zr, 160:320], Z_L)
        push("k_y2r", lambda: kvb.at[y, zr], Y_R)
        push("k_y2l", lambda: kvb.at[y, zr], Y_L)

    def k3():
        got("k_oyr", kvb.at[yo, z, 0:160])
        got("k_oyl", kvb.at[yo, z, 160:320])
        push("k_pzr", lambda: kvb.at[yo, z], Z_R)
        push("k_pzl", lambda: kvb.at[yo, z], Z_L)
        got("k_ozr", kvb.at[y, zo, 0:160])
        got("k_ozl", kvb.at[y, zo, 160:320])
        push("k_y3r", lambda: kvb.at[y, zo], Y_R)
        push("k_y3l", lambda: kvb.at[y, zo], Y_L)

    def k7():
        got("k_y1r", kvb.at[yl, zl])
        got("k_y1l", kvb.at[yr, zl])

    def k9():
        got("k_y2r", kvb.at[yl, zr])
        got("k_y2l", kvb.at[yr, zr])
        got("k_pzr", kvb.at[yo, zl])
        push("k_pozr", lambda: kvb.at[yo, zl, 0:160], Z_R)
        got("k_pzl", kvb.at[yo, zr])
        push("k_pozl", lambda: kvb.at[yo, zr, 160:320], Z_L)

    def k13():
        got("k_y3r", kvb.at[yl, zo])
        got("k_y3l", kvb.at[yr, zo])

    def k15():
        got("k_pozr", kvb.at[yo, zo, 0:160])
        got("k_pozl", kvb.at[yo, zo, 160:320])

    def queries_mate():
        got("q", lq.at[1])
        make_queries(
            lq[1], zmate * 4 + y, wq_ref, qgain_ref[...], lowq_ref, highq_ref, q_ref, 1
        )

    def wx(p):
        def go():
            rng = slice(2 * p, 2 * p + 2)
            got(f"w_xr{p}", wo.at[rng, :, xl, c])
            push(f"w_oxr{p}", lambda: wo.at[2 * p, :, xl, c], X_R)
            push(f"w_cl{p}", lambda: wo.at[rng, :, xl, c], CORE)
            got(f"w_xl{p}", wo.at[rng, :, xr, c])
            push(f"w_oxl{p}", lambda: wo.at[2 * p + 1, :, xr, c], X_L)
            push(f"w_cr{p}", lambda: wo.at[rng, :, xr, c], CORE)

        return go

    def wxo(p):
        got(f"w_oxr{p}", wo.at[2 * p, :, xo, c])
        got(f"w_oxl{p}", wo.at[2 * p + 1, :, xo, c])
        push(f"w_co{p}", lambda: wo.at[2 * p : 2 * p + 2, :, xo, c], CORE)

    hfirst = (z // 2) * LOCAL
    b_own, b_mate = sp, zmate * 4 + y

    def send_mate():
        close_heads(acc_ref, 1, att_ref, HEADS)
        push("att", lambda: att_ref.at[HEADS : HEADS + LOCAL], dev(zz=zmate), att_ref.at[pl.ds(hfirst, LOCAL)])

    at_op = {3: (k1,), 6: (k2,), 9: (k3,), 11: (queries_mate,), 21: (k7,), 22: (wx(0),),
             27: (k9,), 40: (k13,), 42: (k15,), 44: (wx(1),), 47: (send_mate,)}

    def op(t, _):
        for when, todo in at_op.items():
            @pl.when(t == when)
            def _(todo=todo):
                for f in todo:
                    f()

        def pick(test, yes, no):
            return no + test.astype(jnp.int32) * (yes - no)

        late = t >= 39
        kind = pick(t < 36, t % 3, pick(late, (3 - (t - 39) // 4) % 3, 2))
        step = pick(t < 36, t // 3, pick(late, 12 + (t - 39) % 4, t - 27))
        step = step - 3 * ((kind == 2) & (t < 36)).astype(jnp.int32)
        live = step >= 0
        step = jnp.maximum(step, 0)
        dy = pick(step < 3, step, pick(step < 6, 0, pick(step == 6, 3, pick(
            step < 11, 1 + (step - 7) % 2, pick(
                step < 13, 3, pick(step < 15, step - 12, 3))))))
        dz = pick(step < 3, 0, pick(step < 6, step - 2, pick(step == 6, 0, pick(
            step < 11, 1 + (step - 7) // 2, pick(step < 13, step - 10, 3)))))
        yy = pick(dy == 0, y, pick(dy == 1, yl, pick(dy == 2, yr, yo)))
        zz = pick(dz == 0, z, pick(dz == 1, zl, pick(dz == 2, zr, zo)))
        b = zz * 4 + yy
        slot = step % 4
        which = pick(kind == 2, 1, 0)
        bq = pick(live, pick(which == 0, b_own, b_mate), -1)

        @pl.when((kind == 0) & (b <= jnp.maximum(b_own, b_mate)))
        def _():
            expand(
                kvb[yy, zz], b, wkt_ref, wv_ref, gk_ref, gr_ref, lowk_ref, highk_ref, kt_ref,
                v_ref, slot,
            )

        @pl.when((kind > 0) & (b < bq))
        def _():
            attend(False, q_ref, kt_ref, v_ref, m_ref, acc_ref, which, slot)

        @pl.when((kind > 0) & (b == bq))
        def _():
            attend(True, q_ref, kt_ref, v_ref, m_ref, acc_ref, which, slot)

        return 0

    lax.fori_loop(0, OPS, op, 0)
    close_heads(acc_ref, 0, att_ref, hfirst)
    for p in range(2):
        wxo(p)
    got("w_c", wo.at[:, :, x, co])
    for p in range(2):
        got(f"w_cl{p}", wo.at[2 * p : 2 * p + 2, :, xl, co])
        got(f"w_cr{p}", wo.at[2 * p : 2 * p + 2, :, xr, co])
        got(f"w_co{p}", wo.at[2 * p : 2 * p + 2, :, xo, co])
    got("att", att_ref.at[pl.ds(LOCAL - hfirst, LOCAL)])
    finish(att_ref, mixed_ref, ogain_ref, wo, out_ref)
    for i, again in sent:
        view = again()
        pltpu.make_async_copy(view, view, ssem.at[i]).wait()
    assert len(names) <= SLOTS


def per_device(
    tokens, in_gain, w_query_down, w_latent_down, w_rope_key, query_latent_gain, latent_gain,
    w_query_up, w_key_up, w_value_up, query_gain, key_gain, out_gain, w_out,
):
    blocks = lax.axis_size("sp")
    tables = [jnp.asarray(t) for t in rope_tables(blocks)]
    qgain = jnp.pad(query_gain, (0, 256 - QK)).reshape(1, 256)
    gains = jnp.broadcast_to(key_gain[:, None], (QK, 256))
    vm = pl.BlockSpec(memory_space=pltpu.VMEM)
    args = (
        tokens.reshape(ROWS, D), in_gain.reshape(1, D), w_query_down, w_latent_down, w_rope_key.T,
        query_latent_gain.reshape(1, QR), latent_gain.reshape(1, KR), w_query_up, w_key_up,
        w_value_up, qgain, gains[:NOPE], gains[NOPE:], out_gain.reshape(1, D), w_out, *tables,
    )
    out = pl.pallas_call(
        kernel,
        out_shape=jax.ShapeDtypeStruct((ROWS, D), BF),
        in_specs=[vm] * len(args),
        out_specs=vm,
        scratch_shapes=[
            pltpu.VMEM((8, 256, QR + KR), BF),
            pltpu.VMEM((2, LOCAL, 4, 96, 256), BF),
            pltpu.VMEM((4, 4, 4, 2, 16, D), BF),
            pltpu.VMEM((4, 4, 320, 256), BF),
            pltpu.VMEM((2, ROWS, QR), BF),
            pltpu.VMEM((8, ROWS, 256), BF),
            pltpu.VMEM((ROWS, QR + KR), F32),
            pltpu.VMEM((LOCAL, QR, 256), BF),
            pltpu.VMEM((LOCAL, KR, NOPE), BF),
            pltpu.VMEM((LOCAL, NOPE, KR), BF),
            pltpu.VMEM((LOCAL, KR, VD), BF),
            pltpu.VMEM((2, LOCAL, ROWS, 256), BF),
            pltpu.VMEM((4, LOCAL, 256, 256), BF),
            pltpu.VMEM((4, LOCAL, 256, 256), BF),
            pltpu.VMEM((2, LOCAL, ROWS, 128), F32),
            pltpu.VMEM((2, LOCAL, ROWS, 256), F32),
            pltpu.VMEM((HEADS + LOCAL, ROWS, VD), BF),
            pltpu.VMEM((ROWS, D), BF),
            pltpu.SemaphoreType.DMA((SLOTS,)),
            pltpu.SemaphoreType.DMA((SLOTS,)),
        ],
        compiler_params=pltpu.CompilerParams(
            vmem_limit_bytes=60 * 1024 * 1024, collective_id=0, has_side_effects=True
        ),
    )(*args)
    return out.reshape(1, ROWS, D)


def solution(mesh):
    in_specs = (
        P("dp", "sp", None), P(), P("dp", None), P("dp", None), P(), P(), P(),
        P("dp", "sp"), P("dp", "sp"), P("dp", "sp"), P(), P(), P(), P(("sp", "dp"), None),
    )
    return jax.shard_map(
        per_device, mesh=mesh, in_specs=in_specs, out_specs=P("dp", "sp", None), check_vma=False
    )
```

time: 317 us -> 108 us (0.34)
  the two profiles are of different devices: /device:TPU:121 before, /device:TPU:24 now
where the time goes in v2:
time: 108 us; the launch traced here: 106 us
  Pallas kernels  101 us (94%)
  local copies, waits for them, and re-layouts  5.67 us (5%)
    pallas_call x1, Pallas kernels, per_device(): pl.pallas_call(kernel, out_shape=jax.ShapeDtypeStruct((ROWS, D), BF), in_...  101 us
    unnamed x5, local copies, waits for them, and re-layouts  3.66 us

profile of v2, /device:TPU:24, one launch (start us, length us, event | category | flops | bytes accessed | tf_op | source)
XLA Modules:
  0.0 106.4 jit_solution(13105735612460046356)
XLA Ops:
  0.0 0.0 copy-start.1
  0.0 0.7 copy-done.1
  0.7 0.0 copy-start
  0.7 0.7 copy-done
  1.4 0.6 pad.4
  1.9 0.0 slice-start
  1.9 0.7 broadcast_in_dim.9.gr_ref
  2.6 0.0 slice-done
  2.6 0.7 broadcast_in_dim.8.gk_ref
  3.4 100.8 %shard_map.172 = bf16[256,2048]{1,0:T(8,128)(2,1)} custom-call(bf16[256,2048]{1,0:T(8,128)(2,1)} %bitcast.9, f32[1,2048]{1,0:T(1,128)} %bitcast.11, bf16[256,512]{1,0:T(8,128)(2,1)} %wqd_ref.1, bf16[256,256]{1,0:T(8,128)(2,1)} %wld_ref.1, bf16[64,2048]{1,0:T(8,128)(2,1)} %bitcast.10, f32[1,512]{1,0:T(1,128)} %bitcast.14, f32[1,256]{1,0:T(1,128)} %bitcast.15, ...), custom_call_target="tpu_custom_call" | custom-call | tf_op jit(solution)/shard_map/pallas_call | solution.py:509
  104.1 2.3 %copy.20 = bf16[1,256,2048]{2,1,0:T(8,128)(2,1)} copy(bf16[1,256,2048]{2,1,0:T(8,128)(2,1)} %bitcast.8) | data formatting | bytes 2097152
  (1 shorter events, 0.0 us)
Async XLA Ops:
  0.0 0.7 copy-start.1
  0.7 0.7 copy-start
  1.9 0.7 slice-start

commit v3 on v2

--- a/solution.py
+++ b/solution.py
@@ -75,23 +75,18 @@
     sine_a = jnp.where(lane < ROPE // 2, -sine, 0.0)
     sine_b = jnp.where(lane < ROPE // 2, 0.0, sine)
 
-    def one(g, _):
-        for i in range(2):
-            h = g * 2 + i
-            q = dot(latq, wq_ref[h])
-            scale = lax.rsqrt(jnp.sum(q * q, axis=1, keepdims=True) * (1.0 / QK) + EPS)
-            n = q * scale * qgain
-            t = n[:, NOPE:256]
-            turned = (
-                t * cosine
-                + pltpu.roll(t, 128 - ROPE // 2, 1) * sine_a
-                + pltpu.roll(t, ROPE // 2, 1) * sine_b
-            )
-            q_ref[which, h, :, 0:NOPE] = n[:, 0:NOPE].astype(BF)
-            q_ref[which, h, :, NOPE:256] = turned.astype(BF)
-        return 0
-
-    lax.fori_loop(0, LOCAL // 2, one, 0)
+    for h in range(LOCAL):
+        q = dot(latq, wq_ref[h])
+        scale = lax.rsqrt(jnp.sum(q * q, axis=1, keepdims=True) * (1.0 / QK) + EPS)
+        n = q * scale * qgain
+        t = n[:, NOPE:256]
+        turned = (
+            t * cosine
+            + pltpu.roll(t, 128 - ROPE // 2, 1) * sine_a
+            + pltpu.roll(t, ROPE // 2, 1) * sine_b
+        )
+        q_ref[which, h, :, 0:NOPE] = n[:, 0:NOPE].astype(BF)
+        q_ref[which, h, :, NOPE:256] = turned.astype(BF)
 
 
 def expand(unit, block, wkt_ref, wv_ref, gk_ref, gr_ref, lowk_ref, highk_ref, kt_ref, v_ref, slot):
@@ -165,15 +160,15 @@
 
 
 SLOTS = 128
-OPS = 51
+KEPT = 5
 
 
 def kernel(
     tok_ref, ing_ref, wqd_ref, wld_ref, wrt_ref, qlg_ref, klg_ref, wqu_ref, wku_ref, wvu_ref,
-    qgain_ref, gk_ref, gr_ref, ogain_ref, wo_in_ref, lowq_ref, highq_ref, lowk_ref, highk_ref,
+    qg_ref, kg_ref, ogain_ref, wo_in_ref, lowq_ref, highq_ref, lowk_ref, highk_ref,
     out_ref,
     wd, us, wo, kvb, lq, normed, sums, wq_ref, wk_ref, wkt_ref, wv_ref, q_ref, kt_ref, v_ref,
-    m_ref, acc_ref, att_ref, mixed_ref, ssem, rsem,
+    m_ref, acc_ref, att_ref, mixed_ref, qgain_ref, gk_ref, gr_ref, ssem, rsem,
 ):
     sp, dp = lax.axis_index("sp"), lax.axis_index("dp")
     z, y = sp // 4, sp % 4
@@ -211,7 +206,8 @@
         pltpu.make_async_copy(view, view, rsem.at[number(name)]).wait()
 
     barrier = pltpu.get_barrier_semaphore()
-    for to in (X_R, X_L, Y_R, Y_L, Z_R, Z_L, CORE):
+    X_O, Y_O = dev(xx=xo), dev(yy=yo)
+    for to in (X_R, X_L, X_O, Y_R, Y_L, Y_O, Z_R, Z_L, CORE):
         pl.semaphore_signal(barrier, 1, device_id=to, device_id_type=pl.DeviceIdType.MESH)
 
     hl = zb * 4 + y
@@ -224,14 +220,16 @@
     wo[z, y, x, c] = wo_in_ref[...]
     wd[dp, :, 0:QR] = wqd_ref[...]
     wd[dp, :, QR : QR + KR] = wld_ref[...]
-    pl.semaphore_wait(barrier, 7)
+    pl.semaphore_wait(barrier, 9)
 
     uown = us.at[c, hl, x]
     push("u_r", uown, X_R)
     push("u_l", uown, X_L)
+    push("u_o", uown, X_O)
     wown = wo.at[z, y, x, c]
     push("w_yr", wown, Y_R)
     push("w_yl", wown, Y_L)
+    push("w_yo", wown, Y_O)
     down = wd.at[dp]
     push("d_r", down, X_R)
     push("d_l", down, X_L)
@@ -243,23 +241,27 @@
         for k in range(8):
             normed[k, rows] = n[:, k * 256 : (k + 1) * 256]
 
+    qgain_ref[:, 0:NOPE] = qg_ref[:, 0:NOPE]
+    qgain_ref[:, NOPE:256] = jnp.concatenate(
+        [qg_ref[:, NOPE:QK], jnp.zeros((1, 256 - QK), F32)], axis=1
+    )
+    kg = jnp.concatenate([kg_ref[...], jnp.zeros((1, 256 - QK), F32)], axis=1)
+    column = jnp.broadcast_to(kg[:, 0:NOPE], (NOPE, NOPE)).T
+    gk_ref[...] = jnp.concatenate([column, column], axis=1)
+    column = jnp.broadcast_to(kg[:, NOPE:256], (NOPE, NOPE)).T[0:ROPE]
+    gr_ref[...] = jnp.concatenate([column, column], axis=1)
+
     got("u_r", us.at[c, hl, xl])
-    push("u_or", us.at[c, hl, xl, 0:48], X_R)
     got("u_l", us.at[c, hl, xr])
-    push("u_ol", us.at[c, hl, xr, 48:96], X_L)
-    got("w_yr", wo.at[z, yl, x, c])
-    push("w_oyr", wo.at[z, yl, x, c, :, 0:1024], Y_R)
-    got("w_yl", wo.at[z, yr, x, c])
-    push("w_oyl", wo.at[z, yr, x, c, :, 1024:2048], Y_L)
-    got("u_or", us.at[c, hl, xo, 0:48])
-    got("u_ol", us.at[c, hl, xo, 48:96])
+    got("u_o", us.at[c, hl, xo])
     block0 = us.at[c, hl]
     push("u_z", block0, dev(zz=zpair))
     push("u_y0r", block0, Y_R)
     push("u_y0l", block0, Y_L)
     push("u_c0", block0, CORE)
-    got("w_oyr", wo.at[z, yo, x, c, :, 0:1024])
-    got("w_oyl", wo.at[z, yo, x, c, :, 1024:2048])
+    got("w_yr", wo.at[z, yl, x, c])
+    got("w_yl", wo.at[z, yr, x, c])
+    got("w_yo", wo.at[z, yo, x, c])
     push("w_zr", wo.at[z, :, x, c], Z_R)
     push("w_zl", wo.at[z, :, x, c], Z_L)
 
@@ -273,10 +275,16 @@
     add(dp, True)
     got("d_c", wd.at[2 * x + co])
     add(2 * x + co)
+    m_ref[...] = jnp.full(m_ref.shape, NEG_BIG, F32)
+    acc_ref[...] = jnp.zeros(acc_ref.shape, F32)
+    kt_ref[:, :, QK:256, :] = jnp.zeros((KEPT, LOCAL, 256 - QK, 256), BF)
+    v_ref[:, :, :, VD:256] = jnp.ones((KEPT, LOCAL, ROWS, 256 - VD), BF)
+    rope_t = jnp.zeros((ROPE, ROWS), F32)
+    for k in range(8):
+        rope_t = rope_t + dot_nt(wrt_ref[:, k * 256 : (k + 1) * 256], normed[k])
+    kvb[y, z, 256:320] = rope_t.astype(BF)
     base0, base1 = zb * 4, 4 - zb * 4
-    got("u_z", us.at[c, base1 + y])
     block1 = us.at[c, base1 + y]
-    push("u_c1", block1, CORE)
 
     def ring_y(j, base):
         got(f"u_y{j}r", us.at[c, base + yl])
@@ -287,8 +295,10 @@
         push(f"u_c{j}r", us.at[c, base + yr], CORE)
 
     ring_y(0, base0)
+    got("u_z", us.at[c, base1 + y])
     push("u_y1r", block1, Y_R)
     push("u_y1l", block1, Y_L)
+    push("u_c1", block1, CORE)
     got("d_r", wd.at[2 * xl + c])
     push("d_or", wd.at[2 * xl + c, 0:128], X_R)
     push("d_cl", wd.at[2 * xl + c], CORE)
@@ -310,16 +320,12 @@
     push("d_coa", wd.at[2 * xo + c, 0:128], CORE)
     got("d_ol", wd.at[2 * xo + c, 128:256])
     push("d_cob", wd.at[2 * xo + c, 128:256], CORE)
-    rope_t = jnp.zeros((ROPE, ROWS), F32)
-    for k in range(8):
-        rope_t = rope_t + dot_nt(wrt_ref[:, k * 256 : (k + 1) * 256], normed[k])
     add(2 * xo + c)
     got("d_coa", wd.at[2 * xo + co, 0:128])
     got("d_cob", wd.at[2 * xo + co, 128:256])
     add(2 * xo + co)
 
     kvb[y, z, 0:256] = rms_rows(sums[:, QR : QR + KR], klg_ref[...]).astype(BF)
-    kvb[y, z, 256:320] = rope_t.astype(BF)
     lq[0] = rms_rows(sums[:, 0:QR], qlg_ref[...]).astype(BF)
     own = kvb.at[y, z]
     push("k_yr", own, Y_R)
@@ -346,11 +352,6 @@
     prepare_up(us, wq_ref, wk_ref, wv_ref)
     transpose_keys(wk_ref, wkt_ref)
     make_queries(lq[0], sp, wq_ref, qgain_ref[...], lowq_ref, highq_ref, q_ref, 0)
-    m_ref[...] = jnp.full(m_ref.shape, NEG_BIG, F32)
-    acc_ref[...] = jnp.zeros(acc_ref.shape, F32)
-    kt_ref[:, :, QK:256, :] = jnp.zeros((4, LOCAL, 256 - QK, 256), BF)
-    v_ref[:, :, :, VD:256] = jnp.ones((4, LOCAL, ROWS, 256 - VD), BF)
-
     def k1():
         got("k_yr", kvb.at[yl, z])
         push("k_oyr", lambda: kvb.at[yl, z, 0:160], Y_R)
@@ -427,25 +428,10 @@
         close_heads(acc_ref, 1, att_ref, HEADS)
         push("att", lambda: att_ref.at[HEADS : HEADS + LOCAL], dev(zz=zmate), att_ref.at[pl.ds(hfirst, LOCAL)])
 
-    at_op = {3: (k1,), 6: (k2,), 9: (k3,), 11: (queries_mate,), 21: (k7,), 22: (wx(0),),
-             27: (k9,), 40: (k13,), 42: (k15,), 44: (wx(1),), 47: (send_mate,)}
-
-    def op(t, _):
-        for when, todo in at_op.items():
-            @pl.when(t == when)
-            def _(todo=todo):
-                for f in todo:
-                    f()
-
-        def pick(test, yes, no):
-            return no + test.astype(jnp.int32) * (yes - no)
-
-        late = t >= 39
-        kind = pick(t < 36, t % 3, pick(late, (3 - (t - 39) // 4) % 3, 2))
-        step = pick(t < 36, t // 3, pick(late, 12 + (t - 39) % 4, t - 27))
-        step = step - 3 * ((kind == 2) & (t < 36)).astype(jnp.int32)
-        live = step >= 0
-        step = jnp.maximum(step, 0)
+    def pick(test, yes, no):
+        return no + test.astype(jnp.int32) * (yes - no)
+
+    def source(step):
         dy = pick(step < 3, step, pick(step < 6, 0, pick(step == 6, 3, pick(
             step < 11, 1 + (step - 7) % 2, pick(
                 step < 13, 3, pick(step < 15, step - 12, 3))))))
@@ -453,29 +439,74 @@
             step < 11, 1 + (step - 7) // 2, pick(step < 13, step - 10, 3)))))
         yy = pick(dy == 0, y, pick(dy == 1, yl, pick(dy == 2, yr, yo)))
         zz = pick(dz == 0, z, pick(dz == 1, zl, pick(dz == 2, zr, zo)))
-        b = zz * 4 + yy
-        slot = step % 4
-        which = pick(kind == 2, 1, 0)
-        bq = pick(live, pick(which == 0, b_own, b_mate), -1)
-
-        @pl.when((kind == 0) & (b <= jnp.maximum(b_own, b_mate)))
+        return yy, zz, zz * 4 + yy
+
+    b_last = jnp.maximum(b_own, b_mate)
+
+    def expand_step(step, slot):
+        yy, zz, b = source(step)
+
+        @pl.when(b <= b_last)
         def _():
             expand(
                 kvb[yy, zz], b, wkt_ref, wv_ref, gk_ref, gr_ref, lowk_ref, highk_ref, kt_ref,
                 v_ref, slot,
             )
 
-        @pl.when((kind > 0) & (b < bq))
+    def attend_step(step, slot, which, bq, diagonal=False):
+        b = source(step)[2]
+
+        @pl.when(b == bq if diagonal else b < bq)
         def _():
-            attend(False, q_ref, kt_ref, v_ref, m_ref, acc_ref, which, slot)
-
-        @pl.when((kind > 0) & (b == bq))
+            attend(diagonal, q_ref, kt_ref, v_ref, m_ref, acc_ref, which, slot)
+
+    def start(step, _):
+        @pl.when(step == 1)
         def _():
-            attend(True, q_ref, kt_ref, v_ref, m_ref, acc_ref, which, slot)
-
-        return 0
-
-    lax.fori_loop(0, OPS, op, 0)
+            k1()
+
+        expand_step(step, step)
+        attend_step(step, step, 0, b_own, True)
+        return 0
+
+    lax.fori_loop(0, 3, start, 0)
+    k2()
+    queries_mate()
+
+    def mate_start(step, _):
+        attend_step(step, step, 1, b_mate)
+        return 0
+
+    lax.fori_loop(0, 3, mate_start, 0)
+    k3()
+    at_step = {5: (k7,), 7: (wx(0),), 8: (k9,), 12: (k13,), 13: (wx(1),), 15: (k15,)}
+
+    def middle(step, _):
+        for when, todo in at_step.items():
+            @pl.when(step == when)
+            def _(todo=todo):
+                for f in todo:
+                    f()
+
+        slot = pick(step == 6, 3, 4)
+        expand_step(step, slot)
+
+        @pl.when(step != 6)
+        def _():
+            attend_step(step, slot, 0, b_own)
+
+        attend_step(step, slot, 1, b_mate)
+        attend_step(step, slot, 1, b_mate, True)
+        return 0
+
+    lax.fori_loop(3, 16, middle, 0)
+    send_mate()
+
+    def last(i, _):
+        attend_step(pick(i == 3, 6, i), i, 0, b_own)
+        return 0
+
+    lax.fori_loop(1, 4, last, 0)
     close_heads(acc_ref, 0, att_ref, hfirst)
     for p in range(2):
         wxo(p)
@@ -498,13 +529,11 @@
 ):
     blocks = lax.axis_size("sp")
     tables = [jnp.asarray(t) for t in rope_tables(blocks)]
-    qgain = jnp.pad(query_gain, (0, 256 - QK)).reshape(1, 256)
-    gains = jnp.broadcast_to(key_gain[:, None], (QK, 256))
     vm = pl.BlockSpec(memory_space=pltpu.VMEM)
     args = (
         tokens.reshape(ROWS, D), in_gain.reshape(1, D), w_query_down, w_latent_down, w_rope_key.T,
         query_latent_gain.reshape(1, QR), latent_gain.reshape(1, KR), w_query_up, w_key_up,
-        w_value_up, qgain, gains[:NOPE], gains[NOPE:], out_gain.reshape(1, D), w_out, *tables,
+        w_value_up, query_gain.reshape(1, QK), key_gain.reshape(1, QK), out_gain.reshape(1, D), w_out, *tables,
     )
     out = pl.pallas_call(
         kernel,
@@ -524,12 +553,15 @@
             pltpu.VMEM((LOCAL, NOPE, KR), BF),
             pltpu.VMEM((LOCAL, KR, VD), BF),
             pltpu.VMEM((2, LOCAL, ROWS, 256), BF),
-            pltpu.VMEM((4, LOCAL, 256, 256), BF),
-            pltpu.VMEM((4, LOCAL, 256, 256), BF),
+            pltpu.VMEM((KEPT, LOCAL, 256, 256), BF),
+            pltpu.VMEM((KEPT, LOCAL, 256, 256), BF),
             pltpu.VMEM((2, LOCAL, ROWS, 128), F32),
             pltpu.VMEM((2, LOCAL, ROWS, 256), F32),
             pltpu.VMEM((HEADS + LOCAL, ROWS, VD), BF),
             pltpu.VMEM((ROWS, D), BF),
+            pltpu.VMEM((1, 256), F32),
+            pltpu.VMEM((NOPE, 256), F32),
+            pltpu.VMEM((ROPE, 256), F32),
             pltpu.SemaphoreType.DMA((SLOTS,)),
             pltpu.SemaphoreType.DMA((SLOTS,)),
         ],

time: 108 us -> 88.8 us (0.82)
  Pallas kernels: 101 us -> 85.4 us
  local copies, waits for them, and re-layouts: 5.67 us -> 2.3 us
    pallas_call x1, Pallas kernels: 101 us -> 85.4 us  [per_device(): pl.pallas_call(kernel, out_shape=jax.ShapeDtypeStruct((ROWS, D), BF), in_...]
    broadcast_in_dim x2 -> x0, local copies, waits for them, and re-layouts: 1.43 us -> none  [per_device(): gains = jnp.broadcast_to(key_gain[:, None], (QK, 256))]
    unnamed x5 -> x1, local copies, waits for them, and re-layouts: 3.66 us -> 2.3 us
where the time goes in v3:
time: 88.8 us; the launch traced here: 87.7 us
  Pallas kernels  85.4 us (96%)
  local copies, waits for them, and re-layouts  2.3 us (3%)
    pallas_call x1, Pallas kernels, per_device(): pl.pallas_call(kernel, out_shape=jax.ShapeDtypeStruct((ROWS, D), BF), in_...  85.4 us
    unnamed x1, local copies, waits for them, and re-layouts  2.3 us

profile of v3, /device:TPU:24, one launch (start us, length us, event | category | flops | bytes accessed | tf_op | source)
XLA Modules:
  0.0 87.7 jit_solution(9764399359260449518)
XLA Ops:
  0.0 85.4 %shard_map.172 = bf16[256,2048]{1,0:T(8,128)(2,1)} custom-call(bf16[256,2048]{1,0:T(8,128)(2,1)} %bitcast.10, f32[1,2048]{1,0:T(1,128)} %bitcast.12, bf16[256,512]{1,0:T(8,128)(2,1)} %wqd_ref.1, bf16[256,256]{1,0:T(8,128)(2,1)} %wld_ref.1, bf16[64,2048]{1,0:T(8,128)(2,1)} %bitcast.11, f32[1,512]{1,0:T(1,128)} %bitcast.14, f32[1,256]{1,0:T(1,128)} %bitcast.15, ...), custom_call_target="tpu_custom_call" | custom-call | tf_op jit(solution)/shard_map/pallas_call | solution.py:538
  85.4 2.3 %copy.20 = bf16[1,256,2048]{2,1,0:T(8,128)(2,1)} copy(bf16[1,256,2048]{2,1,0:T(8,128)(2,1)} %bitcast.9) | data formatting | bytes 2097152

commit v4 on v3

--- a/solution.py
+++ b/solution.py
@@ -43,16 +43,19 @@
     return lax.dot_general(a, b, (((1,), (1,)), ((), ())), preferred_element_type=F32)
 
 
-def prepare_up(us, wq_ref, wkt_ref, wv_ref):
+def prepare_up(us, wq_ref, wk_ref, wv_ref):
     def one(h, _):
         for x in range(4):
             for c in range(2):
                 d = 2 * x + c
                 unit = us[c, h, x]
-                wq_ref[h, d * 64 : d * 64 + 64] = unit[0:64]
+                rows = slice(d * 64, d * 64 + 64)
+                wq_ref[h, rows, 0:NOPE] = unit[0:64]
+                wq_ref[h, d * 64 : d * 64 + 32, NOPE:QK] = unit[64:96, 0:ROPE]
+                wq_ref[h, d * 64 + 32 : d * 64 + 64, NOPE:QK] = unit[64:96, ROPE:128]
                 kv_rows = slice(d * 32, d * 32 + 32)
-                wv_ref[h, kv_rows] = unit[64:96, NOPE:256]
-                wkt_ref[h, kv_rows] = unit[64:96, 0:NOPE]
+                wk_ref[h, kv_rows] = unit[96:128]
+                wv_ref[h, kv_rows] = unit[128:160]
         return 0
 
     lax.fori_loop(0, LOCAL, one, 0)
@@ -147,12 +150,12 @@
         mixed_ref[:, cols] = (att_ref[h].astype(F32) * scale * ogain_ref[:, cols]).astype(BF)
 
     def one(j, _):
-        cols = pl.ds(pl.multiple_of(j * 256, 256), 256)
-        w = wo_ref[:, :, :, :, :, cols].reshape(HEADS * VD, 256)
+        cols = pl.ds(pl.multiple_of(j * 512, 512), 512)
+        w = wo_ref[:, :, :, :, :, cols].reshape(HEADS * VD, 512)
         out_ref[:, cols] = dot(mixed_ref[...], w).astype(BF)
         return 0
 
-    lax.fori_loop(0, D // 256, one, 0)
+    lax.fori_loop(0, D // 512, one, 0)
 
 
 def rms_rows(values, scaling):
@@ -160,7 +163,7 @@
 
 
 SLOTS = 128
-KEPT = 5
+KEPT = 2
 
 
 def kernel(
@@ -211,12 +214,12 @@
         pl.semaphore_signal(barrier, 1, device_id=to, device_id_type=pl.DeviceIdType.MESH)
 
     hl = zb * 4 + y
-    us[c, hl, x, 0:64, 0:NOPE] = wqu_ref[:, 0:NOPE]
-    us[c, hl, x, 0:64, NOPE:256] = jnp.concatenate(
-        [wqu_ref[:, NOPE:QK], jnp.zeros((64, 256 - QK), BF)], axis=1
+    us[c, hl, x, 0:64] = wqu_ref[:, 0:NOPE]
+    us[c, hl, x, 64:96] = jnp.concatenate(
+        [wqu_ref[0:32, NOPE:QK], wqu_ref[32:64, NOPE:QK]], axis=1
     )
-    us[c, hl, x, 64:96, 0:NOPE] = wku_ref[...]
-    us[c, hl, x, 64:96, NOPE:256] = wvu_ref[...]
+    us[c, hl, x, 96:128] = wku_ref[...]
+    us[c, hl, x, 128:160] = wvu_ref[...]
     wo[z, y, x, c] = wo_in_ref[...]
     wd[dp, :, 0:QR] = wqd_ref[...]
     wd[dp, :, QR : QR + KR] = wld_ref[...]
@@ -277,6 +280,7 @@
     add(2 * x + co)
     m_ref[...] = jnp.full(m_ref.shape, NEG_BIG, F32)
     acc_ref[...] = jnp.zeros(acc_ref.shape, F32)
+    wq_ref[:, :, QK:256] = jnp.zeros((LOCAL, QR, 256 - QK), BF)
     kt_ref[:, :, QK:256, :] = jnp.zeros((KEPT, LOCAL, 256 - QK, 256), BF)
     v_ref[:, :, :, VD:256] = jnp.ones((KEPT, LOCAL, ROWS, 256 - VD), BF)
     rope_t = jnp.zeros((ROPE, ROWS), F32)
@@ -311,11 +315,19 @@
     add(2 * xl + co)
     got("d_cr", wd.at[2 * xr + co])
     add(2 * xr + co)
+    zrow = (z, zl, zr, zo)
+
+    def row(k):
+        push(f"w_xr{k}", wo.at[zrow[k], :, x, c], X_R)
+        push(f"w_xl{k}", wo.at[zrow[k], :, x, c], X_L)
+
+    row(0)
     got("w_zr", wo.at[zl, :, x, c])
     push("w_ozr", wo.at[zl, 0:2, x, c], Z_R)
     got("w_zl", wo.at[zr, :, x, c])
     push("w_ozl", wo.at[zr, 2:4, x, c], Z_L)
-    ring_y(1, base1)
+    row(1)
+    row(2)
     got("d_or", wd.at[2 * xo + c, 0:128])
     push("d_coa", wd.at[2 * xo + c, 0:128], CORE)
     got("d_ol", wd.at[2 * xo + c, 128:256])
@@ -325,24 +337,23 @@
     got("d_cob", wd.at[2 * xo + co, 128:256])
     add(2 * xo + co)
 
+    lq[0] = rms_rows(sums[:, 0:QR], qlg_ref[...]).astype(BF)
+    push("q", lq.at[0], dev(zz=zmate), lq.at[1])
     kvb[y, z, 0:256] = rms_rows(sums[:, QR : QR + KR], klg_ref[...]).astype(BF)
-    lq[0] = rms_rows(sums[:, 0:QR], qlg_ref[...]).astype(BF)
     own = kvb.at[y, z]
     push("k_yr", own, Y_R)
     push("k_yl", own, Y_L)
     push("k_zr", own, Z_R)
     push("k_zl", own, Z_L)
-    push("q", lq.at[0], dev(zz=zmate), lq.at[1])
-
+
+    ring_y(1, base1)
     for j, base in ((0, base0), (1, base1)):
         got(f"u_y{j}or", us.at[c, base + yo, 0:2])
         got(f"u_y{j}ol", us.at[c, base + yo, 2:4])
         push(f"u_c{j}o", us.at[c, base + yo], CORE)
     got("w_ozr", wo.at[zo, 0:2, x, c])
     got("w_ozl", wo.at[zo, 2:4, x, c])
-    for p in range(2):
-        push(f"w_xr{p}", wo.at[2 * p : 2 * p + 2, :, x, c], X_R)
-        push(f"w_xl{p}", wo.at[2 * p : 2 * p + 2, :, x, c], X_L)
+    row(3)
     for j, base in ((0, base0), (1, base1)):
         got(f"u_c{j}", us.at[co, base + y])
         got(f"u_c{j}l", us.at[co, base + yl])
@@ -385,6 +396,8 @@
     def k9():
         got("k_y2r", kvb.at[yl, zr])
         got("k_y2l", kvb.at[yr, zr])
+
+    def k11():
         got("k_pzr", kvb.at[yo, zl])
         push("k_pozr", lambda: kvb.at[yo, zl, 0:160], Z_R)
         got("k_pzl", kvb.at[yo, zr])
@@ -404,22 +417,23 @@
             lq[1], zmate * 4 + y, wq_ref, qgain_ref[...], lowq_ref, highq_ref, q_ref, 1
         )
 
-    def wx(p):
+    def wx(k):
         def go():
-            rng = slice(2 * p, 2 * p + 2)
-            got(f"w_xr{p}", wo.at[rng, :, xl, c])
-            push(f"w_oxr{p}", lambda: wo.at[2 * p, :, xl, c], X_R)
-            push(f"w_cl{p}", lambda: wo.at[rng, :, xl, c], CORE)
-            got(f"w_xl{p}", wo.at[rng, :, xr, c])
-            push(f"w_oxl{p}", lambda: wo.at[2 * p + 1, :, xr, c], X_L)
-            push(f"w_cr{p}", lambda: wo.at[rng, :, xr, c], CORE)
+            r = zrow[k]
+            got(f"w_xr{k}", wo.at[r, :, xl, c])
+            push(f"w_oxr{k}", lambda: wo.at[r, 0:2, xl, c], X_R)
+            push(f"w_cl{k}", lambda: wo.at[r, :, xl, c], CORE)
+            got(f"w_xl{k}", wo.at[r, :, xr, c])
+            push(f"w_oxl{k}", lambda: wo.at[r, 2:4, xr, c], X_L)
+            push(f"w_cr{k}", lambda: wo.at[r, :, xr, c], CORE)
 
         return go
 
-    def wxo(p):
-        got(f"w_oxr{p}", wo.at[2 * p, :, xo, c])
-        got(f"w_oxl{p}", wo.at[2 * p + 1, :, xo, c])
-        push(f"w_co{p}", lambda: wo.at[2 * p : 2 * p + 2, :, xo, c], CORE)
+    def wxo(k):
+        r = zrow[k]
+        got(f"w_oxr{k}", wo.at[r, 0:2, xo, c])
+        got(f"w_oxl{k}", wo.at[r, 2:4, xo, c])
+        push(f"w_co{k}", wo.at[r, :, xo, c], CORE)
 
     hfirst = (z // 2) * LOCAL
     b_own, b_mate = sp, zmate * 4 + y
@@ -445,76 +459,85 @@
 
     def expand_step(step, slot):
         yy, zz, b = source(step)
-
-        @pl.when(b <= b_last)
-        def _():
-            expand(
-                kvb[yy, zz], b, wkt_ref, wv_ref, gk_ref, gr_ref, lowk_ref, highk_ref, kt_ref,
-                v_ref, slot,
-            )
-
-    def attend_step(step, slot, which, bq, diagonal=False):
-        b = source(step)[2]
-
-        @pl.when(b == bq if diagonal else b < bq)
-        def _():
-            attend(diagonal, q_ref, kt_ref, v_ref, m_ref, acc_ref, which, slot)
-
-    def start(step, _):
-        @pl.when(step == 1)
-        def _():
-            k1()
-
-        expand_step(step, step)
-        attend_step(step, step, 0, b_own, True)
-        return 0
-
-    lax.fori_loop(0, 3, start, 0)
-    k2()
+        expand(
+            kvb[yy, zz], b, wkt_ref, wv_ref, gk_ref, gr_ref, lowk_ref, highk_ref, kt_ref,
+            v_ref, slot,
+        )
+
+    def attend_to(which, slot, diagonal=False):
+        attend(diagonal, q_ref, kt_ref, v_ref, m_ref, acc_ref, which, slot)
+
+    expand_step(jnp.minimum(z, 0), 0)
+    attend_to(0, 0, True)
     queries_mate()
-
-    def mate_start(step, _):
-        attend_step(step, step, 1, b_mate)
-        return 0
-
-    lax.fori_loop(0, 3, mate_start, 0)
-    k3()
-    at_step = {5: (k7,), 7: (wx(0),), 8: (k9,), 12: (k13,), 13: (wx(1),), 15: (k15,)}
-
-    def middle(step, _):
-        for when, todo in at_step.items():
-            @pl.when(step == when)
+    at_pair = {0: (k1, wx(0)), 1: (k2,), 2: (k3, wx(1)), 3: (k7, k11), 4: (k9, wx(2)), 6: (k13,),
+               7: (k15, wx(3))}
+
+    def pair(i, _):
+        for when, todo in at_pair.items():
+            @pl.when(i == when)
             def _(todo=todo):
                 for f in todo:
                     f()
 
-        slot = pick(step == 6, 3, 4)
-        expand_step(step, slot)
-
-        @pl.when(step != 6)
+        first = pick(i == 7, 0, 2 * i + 1)
+        second = pick(i == 7, 15, 2 * i + 2)
+        b0, b1 = source(first)[2], source(second)[2]
+        own_both = (b0 < b_own) & (b1 < b_own)
+        mate_both = (b0 < b_mate) & (b1 < b_mate)
+        either = own_both | mate_both
+        needed = (b0 <= b_last) | (b1 <= b_last)
+        lead = pick(own_both, 0, 1)
+
+        @pl.when(either)
         def _():
-            attend_step(step, slot, 0, b_own)
-
-        attend_step(step, slot, 1, b_mate)
-        attend_step(step, slot, 1, b_mate, True)
+            expand_step(first, 0)
+            expand_step(second, 1)
+            attend_to(lead, 0)
+            attend_to(lead, 1)
+
+        @pl.when(jnp.logical_not(either) & needed)
+        def _():
+            expand_step(first, 0)
+            expand_step(second, 1)
+
+        @pl.when(own_both & mate_both)
+        def _():
+            attend_to(1, 0)
+            attend_to(1, 1)
+
+        def single(j, _):
+            which, slot = j // 2, j % 2
+            b = pick(slot == 0, b0, b1)
+            bq = pick(which == 0, b_own, b_mate)
+            done = pick(which == 0, own_both.astype(jnp.int32), mate_both.astype(jnp.int32))
+
+            @pl.when((b < bq) & (done == 0))
+            def _():
+                attend_to(which, slot)
+
+            @pl.when((b == bq) & (which == 1))
+            def _():
+                attend_to(which, slot, True)
+
+            return 0
+
+        @pl.when(jnp.logical_not(own_both & mate_both))
+        def _():
+            lax.fori_loop(0, 4, single, 0)
+
         return 0
 
-    lax.fori_loop(3, 16, middle, 0)
+    lax.fori_loop(0, 8, pair, 0)
     send_mate()
-
-    def last(i, _):
-        attend_step(pick(i == 3, 6, i), i, 0, b_own)
-        return 0
-
-    lax.fori_loop(1, 4, last, 0)
     close_heads(acc_ref, 0, att_ref, hfirst)
-    for p in range(2):
-        wxo(p)
+    for k in range(4):
+        wxo(k)
     got("w_c", wo.at[:, :, x, co])
-    for p in range(2):
-        got(f"w_cl{p}", wo.at[2 * p : 2 * p + 2, :, xl, co])
-        got(f"w_cr{p}", wo.at[2 * p : 2 * p + 2, :, xr, co])
-        got(f"w_co{p}", wo.at[2 * p : 2 * p + 2, :, xo, co])
+    for k in range(4):
+        got(f"w_cl{k}", wo.at[zrow[k], :, xl, co])
+        got(f"w_cr{k}", wo.at[zrow[k], :, xr, co])
+        got(f"w_co{k}", wo.at[zrow[k], :, xo, co])
     got("att", att_ref.at[pl.ds(LOCAL - hfirst, LOCAL)])
     finish(att_ref, mixed_ref, ogain_ref, wo, out_ref)
     for i, again in sent:
@@ -542,7 +565,7 @@
         out_specs=vm,
         scratch_shapes=[
             pltpu.VMEM((8, 256, QR + KR), BF),
-            pltpu.VMEM((2, LOCAL, 4, 96, 256), BF),
+            pltpu.VMEM((2, LOCAL, 4, 160, 128), BF),
             pltpu.VMEM((4, 4, 4, 2, 16, D), BF),
             pltpu.VMEM((4, 4, 320, 256), BF),
             pltpu.VMEM((2, ROWS, QR), BF),

time: 88.8 us -> 92.8 us (1.045)
  Pallas kernels: 85.4 us -> 89.4 us
    pallas_call x1, Pallas kernels: 85.4 us -> 89.4 us  [per_device(): pl.pallas_call(kernel, out_shape=jax.ShapeDtypeStruct((ROWS, D), BF), in_...]
where the time goes in v4:
time: 92.8 us; the launch traced here: 91.7 us
  Pallas kernels  89.4 us (96%)
  local copies, waits for them, and re-layouts  2.3 us (2%)
    pallas_call x1, Pallas kernels, per_device(): pl.pallas_call(kernel, out_shape=jax.ShapeDtypeStruct((ROWS, D), BF), in_...  89.4 us
    unnamed x1, local copies, waits for them, and re-layouts  2.3 us

profile of v4, /device:TPU:24, one launch (start us, length us, event | category | flops | bytes accessed | tf_op | source)
XLA Modules:
  0.0 91.7 jit_solution(5017269531904767113)
XLA Ops:
  0.0 89.4 %shard_map.172 = bf16[256,2048]{1,0:T(8,128)(2,1)} custom-call(bf16[256,2048]{1,0:T(8,128)(2,1)} %bitcast.10, f32[1,2048]{1,0:T(1,128)} %bitcast.12, bf16[256,512]{1,0:T(8,128)(2,1)} %wqd_ref.1, bf16[256,256]{1,0:T(8,128)(2,1)} %wld_ref.1, bf16[64,2048]{1,0:T(8,128)(2,1)} %bitcast.11, f32[1,512]{1,0:T(1,128)} %bitcast.14, f32[1,256]{1,0:T(1,128)} %bitcast.15, ...), custom_call_target="tpu_custom_call" | custom-call | tf_op jit(solution)/shard_map/pallas_call | solution.py:561
  89.4 2.3 %copy.20 = bf16[1,256,2048]{2,1,0:T(8,128)(2,1)} copy(bf16[1,256,2048]{2,1,0:T(8,128)(2,1)} %bitcast.9) | data formatting | bytes 2097152

commit v5 on v4

--- a/solution.py
+++ b/solution.py
@@ -43,30 +43,19 @@
     return lax.dot_general(a, b, (((1,), (1,)), ((), ())), preferred_element_type=F32)
 
 
-def prepare_up(us, wq_ref, wk_ref, wv_ref):
-    def one(h, _):
-        for x in range(4):
-            for c in range(2):
-                d = 2 * x + c
-                unit = us[c, h, x]
-                rows = slice(d * 64, d * 64 + 64)
-                wq_ref[h, rows, 0:NOPE] = unit[0:64]
-                wq_ref[h, d * 64 : d * 64 + 32, NOPE:QK] = unit[64:96, 0:ROPE]
-                wq_ref[h, d * 64 + 32 : d * 64 + 64, NOPE:QK] = unit[64:96, ROPE:128]
-                kv_rows = slice(d * 32, d * 32 + 32)
-                wk_ref[h, kv_rows] = unit[96:128]
-                wv_ref[h, kv_rows] = unit[128:160]
-        return 0
-
-    lax.fori_loop(0, LOCAL, one, 0)
-
-
-def transpose_keys(wk_ref, wkt_ref):
-    def one(h, _):
-        wkt_ref[h] = wk_ref[h].T
-        return 0
-
-    lax.fori_loop(0, LOCAL, one, 0)
+def prepare_head(us, h, wq_ref, wkt_ref, wv_ref):
+    keys = []
+    for x in range(4):
+        for c in range(2):
+            d = 2 * x + c
+            unit = us[c, h, x]
+            rows = slice(d * 64, d * 64 + 64)
+            wq_ref[h, rows, 0:NOPE] = unit[0:64]
+            wq_ref[h, d * 64 : d * 64 + 32, NOPE:QK] = unit[64:96, 0:ROPE]
+            wq_ref[h, d * 64 + 32 : d * 64 + 64, NOPE:QK] = unit[64:96, ROPE:128]
+            keys.append(unit[96:128])
+            wv_ref[h, d * 32 : d * 32 + 32] = unit[128:160]
+    wkt_ref[h] = jnp.concatenate(keys, axis=0).T
 
 
 def make_queries(latq, block, wq_ref, qgain, lowq_ref, highq_ref, q_ref, which):
@@ -132,6 +121,22 @@
         )
 
 
+def attend_pair(q_ref, kt_ref, v_ref, m_ref, acc_ref, which):
+    for h in range(LOCAL):
+        q = q_ref[which, h]
+        s0, s1 = dot(q, kt_ref[0, h]), dot(q, kt_ref[1, h])
+        old = m_ref[which, h]
+        new = jnp.maximum(old, jnp.max(jnp.maximum(s0, s1), axis=1, keepdims=True))
+        fade = jnp.exp2((old - new) * SOFT)
+        wide = jnp.concatenate([new, new], 1)
+        p0 = jnp.exp2((s0 - wide) * SOFT).astype(BF)
+        p1 = jnp.exp2((s1 - wide) * SOFT).astype(BF)
+        m_ref[which, h] = new
+        acc_ref[which, h] = acc_ref[which, h] * jnp.concatenate([fade, fade], 1) + (
+            dot(p0, v_ref[0, h]) + dot(p1, v_ref[1, h])
+        )
+
+
 def close_heads(acc_ref, which, att_ref, first):
     for h in range(LOCAL):
         att_ref[first + h] = (
@@ -170,7 +175,7 @@
     tok_ref, ing_ref, wqd_ref, wld_ref, wrt_ref, qlg_ref, klg_ref, wqu_ref, wku_ref, wvu_ref,
     qg_ref, kg_ref, ogain_ref, wo_in_ref, lowq_ref, highq_ref, lowk_ref, highk_ref,
     out_ref,
-    wd, us, wo, kvb, lq, normed, sums, wq_ref, wk_ref, wkt_ref, wv_ref, q_ref, kt_ref, v_ref,
+    wd, us, wo, kvb, lq, normed, sums, wq_ref, wkt_ref, wv_ref, q_ref, kt_ref, v_ref,
     m_ref, acc_ref, att_ref, mixed_ref, qgain_ref, gk_ref, gr_ref, ssem, rsem,
 ):
     sp, dp = lax.axis_index("sp"), lax.axis_index("dp")
@@ -298,11 +303,11 @@
         push(f"u_y{j}ol", us.at[c, base + yr, 2:4], Y_L)
         push(f"u_c{j}r", us.at[c, base + yr], CORE)
 
-    ring_y(0, base0)
     got("u_z", us.at[c, base1 + y])
     push("u_y1r", block1, Y_R)
     push("u_y1l", block1, Y_L)
     push("u_c1", block1, CORE)
+    ring_y(0, base0)
     got("d_r", wd.at[2 * xl + c])
     push("d_or", wd.at[2 * xl + c, 0:128], X_R)
     push("d_cl", wd.at[2 * xl + c], CORE)
@@ -328,6 +333,13 @@
     push("w_ozl", wo.at[zr, 2:4, x, c], Z_L)
     row(1)
     row(2)
+    got("u_c0", us.at[co, base0 + y])
+    got("u_c1", us.at[co, base1 + y])
+    got("u_c0l", us.at[co, base0 + yl])
+    got("u_c0r", us.at[co, base0 + yr])
+    for h in (base0 + y, base1 + y, base0 + yl, base0 + yr):
+        prepare_head(us, h, wq_ref, wkt_ref, wv_ref)
+    ring_y(1, base1)
     got("d_or", wd.at[2 * xo + c, 0:128])
     push("d_coa", wd.at[2 * xo + c, 0:128], CORE)
     got("d_ol", wd.at[2 * xo + c, 128:256])
@@ -346,7 +358,6 @@
     push("k_zr", own, Z_R)
     push("k_zl", own, Z_L)
 
-    ring_y(1, base1)
     for j, base in ((0, base0), (1, base1)):
         got(f"u_y{j}or", us.at[c, base + yo, 0:2])
         got(f"u_y{j}ol", us.at[c, base + yo, 2:4])
@@ -354,14 +365,13 @@
     got("w_ozr", wo.at[zo, 0:2, x, c])
     got("w_ozl", wo.at[zo, 2:4, x, c])
     row(3)
-    for j, base in ((0, base0), (1, base1)):
-        got(f"u_c{j}", us.at[co, base + y])
-        got(f"u_c{j}l", us.at[co, base + yl])
-        got(f"u_c{j}r", us.at[co, base + yr])
-        got(f"u_c{j}o", us.at[co, base + yo])
+    got("u_c1l", us.at[co, base1 + yl])
+    got("u_c1r", us.at[co, base1 + yr])
+    got("u_c0o", us.at[co, base0 + yo])
+    got("u_c1o", us.at[co, base1 + yo])
     push("w_c", wo.at[:, :, x, c], CORE)
-    prepare_up(us, wq_ref, wk_ref, wv_ref)
-    transpose_keys(wk_ref, wkt_ref)
+    for h in (base0 + yo, base1 + yl, base1 + yr, base1 + yo):
+        prepare_head(us, h, wq_ref, wkt_ref, wv_ref)
     make_queries(lq[0], sp, wq_ref, qgain_ref[...], lowq_ref, highq_ref, q_ref, 0)
     def k1():
         got("k_yr", kvb.at[yl, z])
@@ -493,8 +503,7 @@
         def _():
             expand_step(first, 0)
             expand_step(second, 1)
-            attend_to(lead, 0)
-            attend_to(lead, 1)
+            attend_pair(q_ref, kt_ref, v_ref, m_ref, acc_ref, lead)
 
         @pl.when(jnp.logical_not(either) & needed)
         def _():
@@ -503,8 +512,7 @@
 
         @pl.when(own_both & mate_both)
         def _():
-            attend_to(1, 0)
-            attend_to(1, 1)
+            attend_pair(q_ref, kt_ref, v_ref, m_ref, acc_ref, 1)
 
         def single(j, _):
             which, slot = j // 2, j % 2
@@ -560,7 +568,7 @@
     )
     out = pl.pallas_call(
         kernel,
-        out_shape=jax.ShapeDtypeStruct((ROWS, D), BF),
+        out_shape=pltpu.VMEM((ROWS, D), BF),
         in_specs=[vm] * len(args),
         out_specs=vm,
         scratch_shapes=[
@@ -572,7 +580,6 @@
             pltpu.VMEM((8, ROWS, 256), BF),
             pltpu.VMEM((ROWS, QR + KR), F32),
             pltpu.VMEM((LOCAL, QR, 256), BF),
-            pltpu.VMEM((LOCAL, KR, NOPE), BF),
             pltpu.VMEM((LOCAL, NOPE, KR), BF),
             pltpu.VMEM((LOCAL, KR, VD), BF),
             pltpu.VMEM((2, LOCAL, ROWS, 256), BF),

time: 92.8 us -> 87.3 us (0.941)
  Pallas kernels: 89.4 us -> 85.5 us
  local copies, waits for them, and re-layouts: 2.3 us -> 0.97 us
    pallas_call x1, Pallas kernels: 89.4 us -> 85.5 us  [per_device(): pl.pallas_call(kernel, out_shape=pltpu.VMEM((ROWS, D), BF), in_specs=[vm]...]
    unnamed x1, local copies, waits for them, and re-layouts: 2.3 us -> 0.97 us
where the time goes in v5:
time: 87.3 us; the launch traced here: 86.4 us
  Pallas kernels  85.5 us (98%)
  local copies, waits for them, and re-layouts  0.97 us (1%)
    pallas_call x1, Pallas kernels, per_device(): pl.pallas_call(kernel, out_shape=pltpu.VMEM((ROWS, D), BF), in_specs=[vm]...  85.5 us

profile of v5, /device:TPU:24, one launch (start us, length us, event | category | flops | bytes accessed | tf_op | source)
XLA Modules:
  0.0 86.4 jit_solution(14910766805178123170)
XLA Ops:
  0.0 85.5 %shard_map.172 = bf16[256,2048]{1,0:T(8,128)(2,1)S(1)} custom-call(bf16[256,2048]{1,0:T(8,128)(2,1)} %bitcast.10, f32[1,2048]{1,0:T(1,128)} %bitcast.12, bf16[256,512]{1,0:T(8,128)(2,1)} %wqd_ref.1, bf16[256,256]{1,0:T(8,128)(2,1)} %wld_ref.1, bf16[64,2048]{1,0:T(8,128)(2,1)} %bitcast.11, f32[1,512]{1,0:T(1,128)} %bitcast.14, f32[1,256]{1,0:T(1,128)} %bitcast.15, ...), custom_call_target="tpu_custom_call" | custom-call | tf_op jit(solution)/shard_map/pallas_call | solution.py:569
  85.5 1.0 %copy.20 = bf16[1,256,2048]{2,1,0:T(8,128)(2,1)} copy(bf16[1,256,2048]{2,1,0:T(8,128)(2,1)S(1)} %bitcast.9) | data formatting | bytes 2097152

commit v6 on v5

--- a/solution.py
+++ b/solution.py
@@ -195,6 +195,8 @@
     X_R, X_L, Y_R, Y_L, Z_R, Z_L, CORE = (
         dev(xx=xr), dev(xx=xl), dev(yy=yr), dev(yy=yl), dev(zz=zr), dev(zz=zl), dev(cc=co)
     )
+    zn, zm = zpair, (z + 3 + 2 * zb) % 4
+    Z_N, Z_M = dev(zz=zn), dev(zz=zm)
     names, sent = {}, []
 
     def number(name):
@@ -239,8 +241,10 @@
     push("w_yl", wown, Y_L)
     push("w_yo", wown, Y_O)
     down = wd.at[dp]
-    push("d_r", down, X_R)
-    push("d_l", down, X_L)
+    push("d_ra", wd.at[dp, 0:128], X_R)
+    push("d_la", wd.at[dp, 128:256], X_L)
+    push("d_rb", wd.at[dp, 128:256], X_R)
+    push("d_lb", wd.at[dp, 0:128], X_L)
     push("d_c", down, CORE)
 
     for r in range(0, ROWS, 64):
@@ -303,16 +307,18 @@
         push(f"u_y{j}ol", us.at[c, base + yr, 2:4], Y_L)
         push(f"u_c{j}r", us.at[c, base + yr], CORE)
 
+    got("d_ra", wd.at[2 * xl + c, 0:128])
+    push("d_or", wd.at[2 * xl + c, 0:128], X_R)
+    got("d_la", wd.at[2 * xr + c, 128:256])
+    push("d_ol", wd.at[2 * xr + c, 128:256], X_L)
     got("u_z", us.at[c, base1 + y])
     push("u_y1r", block1, Y_R)
     push("u_y1l", block1, Y_L)
     push("u_c1", block1, CORE)
     ring_y(0, base0)
-    got("d_r", wd.at[2 * xl + c])
-    push("d_or", wd.at[2 * xl + c, 0:128], X_R)
+    got("d_rb", wd.at[2 * xl + c, 128:256])
     push("d_cl", wd.at[2 * xl + c], CORE)
-    got("d_l", wd.at[2 * xr + c])
-    push("d_ol", wd.at[2 * xr + c, 128:256], X_L)
+    got("d_lb", wd.at[2 * xr + c, 0:128])
     push("d_cr", wd.at[2 * xr + c], CORE)
     add(2 * xl + c)
     add(2 * xr + c)
@@ -355,8 +361,8 @@
     own = kvb.at[y, z]
     push("k_yr", own, Y_R)
     push("k_yl", own, Y_L)
-    push("k_zr", own, Z_R)
-    push("k_zl", own, Z_L)
+    push("k_zn", own, Z_N)
+    push("k_zm", own, Z_M)
 
     for j, base in ((0, base0), (1, base1)):
         got(f"u_y{j}or", us.at[c, base + yo, 0:2])
@@ -373,53 +379,57 @@
     for h in (base0 + yo, base1 + yl, base1 + yr, base1 + yo):
         prepare_head(us, h, wq_ref, wkt_ref, wv_ref)
     make_queries(lq[0], sp, wq_ref, qgain_ref[...], lowq_ref, highq_ref, q_ref, 0)
-    def k1():
+    def k_y():
         got("k_yr", kvb.at[yl, z])
         push("k_oyr", lambda: kvb.at[yl, z, 0:160], Y_R)
         got("k_yl", kvb.at[yr, z])
         push("k_oyl", lambda: kvb.at[yr, z, 160:320], Y_L)
 
-    def k2():
-        got("k_zr", kvb.at[y, zl])
-        push("k_ozr", lambda: kvb.at[y, zl, 0:160], Z_R)
-        push("k_y1r", lambda: kvb.at[y, zl], Y_R)
-        push("k_y1l", lambda: kvb.at[y, zl], Y_L)
-        got("k_zl", kvb.at[y, zr])
-        push("k_ozl", lambda: kvb.at[y, zr, 160:320], Z_L)
-        push("k_y2r", lambda: kvb.at[y, zr], Y_R)
-        push("k_y2l", lambda: kvb.at[y, zr], Y_L)
-
-    def k3():
+    def k_zn():
+        got("k_zn", kvb.at[y, zn])
+        push("k_ozm", lambda: kvb.at[y, zn, 0:160], Z_M)
+        push("k_ynr", lambda: kvb.at[y, zn], Y_R)
+        push("k_ynl", lambda: kvb.at[y, zn], Y_L)
+
+    def k_zm():
+        got("k_zm", kvb.at[y, zm])
+        push("k_ozn", lambda: kvb.at[y, zm, 160:320], Z_N)
+        push("k_ymr", lambda: kvb.at[y, zm], Y_R)
+        push("k_yml", lambda: kvb.at[y, zm], Y_L)
+
+    def k_oy():
         got("k_oyr", kvb.at[yo, z, 0:160])
         got("k_oyl", kvb.at[yo, z, 160:320])
-        push("k_pzr", lambda: kvb.at[yo, z], Z_R)
-        push("k_pzl", lambda: kvb.at[yo, z], Z_L)
-        got("k_ozr", kvb.at[y, zo, 0:160])
-        got("k_ozl", kvb.at[y, zo, 160:320])
-        push("k_y3r", lambda: kvb.at[y, zo], Y_R)
-        push("k_y3l", lambda: kvb.at[y, zo], Y_L)
-
-    def k7():
-        got("k_y1r", kvb.at[yl, zl])
-        got("k_y1l", kvb.at[yr, zl])
-
-    def k9():
-        got("k_y2r", kvb.at[yl, zr])
-        got("k_y2l", kvb.at[yr, zr])
-
-    def k11():
-        got("k_pzr", kvb.at[yo, zl])
-        push("k_pozr", lambda: kvb.at[yo, zl, 0:160], Z_R)
-        got("k_pzl", kvb.at[yo, zr])
-        push("k_pozl", lambda: kvb.at[yo, zr, 160:320], Z_L)
-
-    def k13():
-        got("k_y3r", kvb.at[yl, zo])
-        got("k_y3l", kvb.at[yr, zo])
-
-    def k15():
-        got("k_pozr", kvb.at[yo, zo, 0:160])
-        got("k_pozl", kvb.at[yo, zo, 160:320])
+        push("k_pzn", lambda: kvb.at[yo, z], Z_N)
+        push("k_pzm", lambda: kvb.at[yo, z], Z_M)
+
+    def k_oz():
+        got("k_ozm", kvb.at[y, zo, 0:160])
+        got("k_ozn", kvb.at[y, zo, 160:320])
+        push("k_yor", lambda: kvb.at[y, zo], Y_R)
+        push("k_yol", lambda: kvb.at[y, zo], Y_L)
+
+    def k_pz():
+        got("k_pzn", kvb.at[yo, zn])
+        push("k_pozm", lambda: kvb.at[yo, zn, 0:160], Z_M)
+        got("k_pzm", kvb.at[yo, zm])
+        push("k_pozn", lambda: kvb.at[yo, zm, 160:320], Z_N)
+
+    def k_yn():
+        got("k_ynr", kvb.at[yl, zn])
+        got("k_ynl", kvb.at[yr, zn])
+
+    def k_ym():
+        got("k_ymr", kvb.at[yl, zm])
+        got("k_yml", kvb.at[yr, zm])
+
+    def k_yo():
+        got("k_yor", kvb.at[yl, zo])
+        got("k_yol", kvb.at[yr, zo])
+
+    def k_poz():
+        got("k_pozm", kvb.at[yo, zo, 0:160])
+        got("k_pozn", kvb.at[yo, zo, 160:320])
 
     def queries_mate():
         got("q", lq.at[1])
@@ -456,13 +466,14 @@
         return no + test.astype(jnp.int32) * (yes - no)
 
     def source(step):
-        dy = pick(step < 3, step, pick(step < 6, 0, pick(step == 6, 3, pick(
-            step < 11, 1 + (step - 7) % 2, pick(
-                step < 13, 3, pick(step < 15, step - 12, 3))))))
-        dz = pick(step < 3, 0, pick(step < 6, step - 2, pick(step == 6, 0, pick(
-            step < 11, 1 + (step - 7) // 2, pick(step < 13, step - 10, 3)))))
+        dy = pick(step < 3, step, pick(step < 5, 0, pick(step < 7, step - 4, pick(
+            step == 7, 0, pick(step == 8, 3, pick(step < 11, step - 8, pick(
+                step < 13, 3, pick(step < 15, step - 12, 3))))))))
+        dz = pick(step < 3, 0, pick(step < 5, step - 2, pick(step < 7, 1, pick(
+            step == 7, 3, pick(step == 8, 0, pick(step < 11, 2, pick(
+                step < 13, step - 10, 3)))))))
         yy = pick(dy == 0, y, pick(dy == 1, yl, pick(dy == 2, yr, yo)))
-        zz = pick(dz == 0, z, pick(dz == 1, zl, pick(dz == 2, zr, zo)))
+        zz = pick(dz == 0, z, pick(dz == 1, zn, pick(dz == 2, zm, zo)))
         return yy, zz, zz * 4 + yy
 
     b_last = jnp.maximum(b_own, b_mate)
@@ -477,11 +488,43 @@
     def attend_to(which, slot, diagonal=False):
         attend(diagonal, q_ref, kt_ref, v_ref, m_ref, acc_ref, which, slot)
 
-    expand_step(jnp.minimum(z, 0), 0)
+    def singles(b0, b1, own0, own1, skip_own, skip_mate):
+        def single(j, _):
+            which, slot = j // 2, j % 2
+            b = pick(slot == 0, b0, b1)
+            mine = pick(slot == 0, own0.astype(jnp.int32), own1.astype(jnp.int32)) * (1 - skip_own)
+            mates = (b < b_mate).astype(jnp.int32) * (1 - skip_mate)
+
+            @pl.when(pick(which == 0, mine, mates) == 1)
+            def _():
+                attend_to(which, slot)
+
+            @pl.when((b == b_mate) & (which == 1))
+            def _():
+                attend_to(which, slot, True)
+
+            return 0
+
+        lax.fori_loop(0, 4, single, 0)
+
+    zero = z - z
+    expand_step(zero, 0)
     attend_to(0, 0, True)
+    k_y()
+    k_zn()
+    expand_step(zero + 1, 0)
+    expand_step(zero + 2, 1)
     queries_mate()
-    at_pair = {0: (k1, wx(0)), 1: (k2,), 2: (k3, wx(1)), 3: (k7, k11), 4: (k9, wx(2)), 6: (k13,),
-               7: (k15, wx(3))}
+    k_oy()
+    k_zm()
+    mate_both = (source(zero + 1)[2] < b_mate) & (source(zero + 2)[2] < b_mate)
+
+    @pl.when(mate_both)
+    def _():
+        attend_pair(q_ref, kt_ref, v_ref, m_ref, acc_ref, 1)
+
+    at_pair = {1: (k_oz, wx(0)), 2: (k_yn, k_pz), 3: (wx(1),), 4: (k_ym, wx(2)), 5: (wx(3),),
+               6: (k_yo,), 7: (k_poz,)}
 
     def pair(i, _):
         for when, todo in at_pair.items():
@@ -493,10 +536,12 @@
         first = pick(i == 7, 0, 2 * i + 1)
         second = pick(i == 7, 15, 2 * i + 2)
         b0, b1 = source(first)[2], source(second)[2]
-        own_both = (b0 < b_own) & (b1 < b_own)
+        own0 = (b0 < b_own) & (i > 0) & (first > 0)
+        own1 = (b1 < b_own) & (i > 0) & (second != 8)
+        own_both = own0 & own1
         mate_both = (b0 < b_mate) & (b1 < b_mate)
-        either = own_both | mate_both
-        needed = (b0 <= b_last) | (b1 <= b_last)
+        either = (own_both | mate_both) & (i > 0)
+        needed = ((b0 <= b_last) | (b1 <= b_last)) & (i > 0)
         lead = pick(own_both, 0, 1)
 
         @pl.when(either)
@@ -514,30 +559,26 @@
         def _():
             attend_pair(q_ref, kt_ref, v_ref, m_ref, acc_ref, 1)
 
-        def single(j, _):
-            which, slot = j // 2, j % 2
-            b = pick(slot == 0, b0, b1)
-            bq = pick(which == 0, b_own, b_mate)
-            done = pick(which == 0, own_both.astype(jnp.int32), mate_both.astype(jnp.int32))
-
-            @pl.when((b < bq) & (done == 0))
-            def _():
-                attend_to(which, slot)
-
-            @pl.when((b == bq) & (which == 1))
-            def _():
-                attend_to(which, slot, True)
-
-            return 0
-
         @pl.when(jnp.logical_not(own_both & mate_both))
         def _():
-            lax.fori_loop(0, 4, single, 0)
+            singles(b0, b1, own0, own1, own_both.astype(jnp.int32), mate_both.astype(jnp.int32))
 
         return 0
 
     lax.fori_loop(0, 8, pair, 0)
     send_mate()
+
+    def last(j, _):
+        step = pick(j == 2, 8, j + 1)
+
+        @pl.when(source(step)[2] < b_own)
+        def _():
+            expand_step(step, 0)
+            attend_to(0, 0)
+
+        return 0
+
+    lax.fori_loop(0, 3, last, 0)
     close_heads(acc_ref, 0, att_ref, hfirst)
     for k in range(4):
         wxo(k)

time: 87.3 us -> 85.8 us (0.983)
  no operation moved by 1% of the time
where the time goes in v6:
time: 85.8 us; the launch traced here: 85.7 us
  Pallas kernels  84.7 us (99%)
  local copies, waits for them, and re-layouts  0.97 us (1%)
    pallas_call x1, Pallas kernels, per_device(): pl.pallas_call(kernel, out_shape=pltpu.VMEM((ROWS, D), BF), in_specs=[vm]...  84.7 us

profile of v6, /device:TPU:24, one launch (start us, length us, event | category | flops | bytes accessed | tf_op | source)
XLA Modules:
  0.0 85.7 jit_solution(11156705842474739013)
XLA Ops:
  0.0 84.7 %shard_map.172 = bf16[256,2048]{1,0:T(8,128)(2,1)S(1)} custom-call(bf16[256,2048]{1,0:T(8,128)(2,1)} %bitcast.10, f32[1,2048]{1,0:T(1,128)} %bitcast.12, bf16[256,512]{1,0:T(8,128)(2,1)} %wqd_ref.1, bf16[256,256]{1,0:T(8,128)(2,1)} %wld_ref.1, bf16[64,2048]{1,0:T(8,128)(2,1)} %bitcast.11, f32[1,512]{1,0:T(1,128)} %bitcast.14, f32[1,256]{1,0:T(1,128)} %bitcast.15, ...), custom_call_target="tpu_custom_call" | custom-call | tf_op jit(solution)/shard_map/pallas_call | solution.py:610
  84.7 1.0 %copy.20 = bf16[1,256,2048]{2,1,0:T(8,128)(2,1)} copy(bf16[1,256,2048]{2,1,0:T(8,128)(2,1)S(1)} %bitcast.9) | data formatting | bytes 2097152

commit v7 on v6

--- a/solution.py
+++ b/solution.py
@@ -54,7 +54,7 @@
             wq_ref[h, d * 64 : d * 64 + 32, NOPE:QK] = unit[64:96, 0:ROPE]
             wq_ref[h, d * 64 + 32 : d * 64 + 64, NOPE:QK] = unit[64:96, ROPE:128]
             keys.append(unit[96:128])
-            wv_ref[h, d * 32 : d * 32 + 32] = unit[128:160]
+            wv_ref[h // 2, d * 32 : d * 32 + 32, pl.ds(pl.multiple_of(h % 2 * VD, VD), VD)] = unit[128:160]
     wkt_ref[h] = jnp.concatenate(keys, axis=0).T
 
 
@@ -100,8 +100,10 @@
         scale = lax.rsqrt((jnp.sum(k * k, axis=0, keepdims=True) + rope_sq) * (1.0 / QK) + EPS)
         kt_ref[slot, h, 0:NOPE] = (k * scale * gk_ref[...]).astype(BF)
         kt_ref[slot, h, NOPE:QK] = (turned * scale).astype(BF)
-    for h in range(LOCAL):
-        v_ref[slot, h, :, 0:VD] = dot(kv, wv_ref[h]).astype(BF)
+    for h in range(0, LOCAL, 2):
+        v = dot(kv, wv_ref[h // 2]).astype(BF)
+        v_ref[slot, h, :, 0:VD] = v[:, 0:VD]
+        v_ref[slot, h + 1, :, 0:VD] = v[:, VD : 2 * VD]
 
 
 def attend(diagonal, q_ref, kt_ref, v_ref, m_ref, acc_ref, which, slot):
@@ -172,11 +174,12 @@
 
 
 def kernel(
-    tok_ref, ing_ref, wqd_ref, wld_ref, wrt_ref, qlg_ref, klg_ref, wqu_ref, wku_ref, wvu_ref,
-    qg_ref, kg_ref, ogain_ref, wo_in_ref, lowq_ref, highq_ref, lowk_ref, highk_ref,
+    tok_in, ing_ref, wqd_in, wld_in, wrt_in, qlg_ref, klg_ref, wqu_in, wku_in, wvu_in,
+    qg_ref, kg_ref, ogain_ref, wo_in, lowq_in, highq_in, lowk_in, highk_in,
     out_ref,
     wd, us, wo, kvb, lq, normed, sums, wq_ref, wkt_ref, wv_ref, q_ref, kt_ref, v_ref,
-    m_ref, acc_ref, att_ref, mixed_ref, qgain_ref, gk_ref, gr_ref, ssem, rsem,
+    m_ref, acc_ref, att_ref, mixed_ref, qgain_ref, gk_ref, gr_ref,
+    tok_ref, wrt_ref, wqu_ref, lowq_ref, highq_ref, lowk_ref, highk_ref, lsem, ssem, rsem,
 ):
     sp, dp = lax.axis_index("sp"), lax.axis_index("dp")
     z, y = sp // 4, sp % 4
@@ -221,15 +224,25 @@
         pl.semaphore_signal(barrier, 1, device_id=to, device_id_type=pl.DeviceIdType.MESH)
 
     hl = zb * 4 + y
+    loads = [
+        pltpu.make_async_copy(src, dst, lsem.at[i])
+        for i, (src, dst) in enumerate((
+            (wqu_in, wqu_ref), (wku_in, us.at[c, hl, x, 96:128]),
+            (wvu_in, us.at[c, hl, x, 128:160]), (wo_in, wo.at[z, y, x, c]),
+            (wqd_in, wd.at[dp, :, 0:QR]), (wld_in, wd.at[dp, :, QR : QR + KR]),
+            (tok_in, tok_ref), (wrt_in, wrt_ref), (lowq_in, lowq_ref), (highq_in, highq_ref),
+            (lowk_in, lowk_ref), (highk_in, highk_ref),
+        ))
+    ]
+    for load in loads:
+        load.start()
+    loads[0].wait()
     us[c, hl, x, 0:64] = wqu_ref[:, 0:NOPE]
     us[c, hl, x, 64:96] = jnp.concatenate(
         [wqu_ref[0:32, NOPE:QK], wqu_ref[32:64, NOPE:QK]], axis=1
     )
-    us[c, hl, x, 96:128] = wku_ref[...]
-    us[c, hl, x, 128:160] = wvu_ref[...]
-    wo[z, y, x, c] = wo_in_ref[...]
-    wd[dp, :, 0:QR] = wqd_ref[...]
-    wd[dp, :, QR : QR + KR] = wld_ref[...]
+    for load in loads[1:4]:
+        load.wait()
     pl.semaphore_wait(barrier, 9)
 
     uown = us.at[c, hl, x]
@@ -240,6 +253,8 @@
     push("w_yr", wown, Y_R)
     push("w_yl", wown, Y_L)
     push("w_yo", wown, Y_O)
+    loads[4].wait()
+    loads[5].wait()
     down = wd.at[dp]
     push("d_ra", wd.at[dp, 0:128], X_R)
     push("d_la", wd.at[dp, 128:256], X_L)
@@ -247,6 +262,8 @@
     push("d_lb", wd.at[dp, 0:128], X_L)
     push("d_c", down, CORE)
 
+    for load in loads[6:]:
+        load.wait()
     for r in range(0, ROWS, 64):
         rows = slice(r, r + 64)
         n = rms_rows(tok_ref[rows].astype(F32), ing_ref[...]).astype(BF)
@@ -515,16 +532,14 @@
     expand_step(zero + 1, 0)
     expand_step(zero + 2, 1)
     queries_mate()
-    k_oy()
-    k_zm()
     mate_both = (source(zero + 1)[2] < b_mate) & (source(zero + 2)[2] < b_mate)
 
     @pl.when(mate_both)
     def _():
         attend_pair(q_ref, kt_ref, v_ref, m_ref, acc_ref, 1)
 
-    at_pair = {1: (k_oz, wx(0)), 2: (k_yn, k_pz), 3: (wx(1),), 4: (k_ym, wx(2)), 5: (wx(3),),
-               6: (k_yo,), 7: (k_poz,)}
+    at_pair = {1: (k_oy, k_zm, wx(0)), 2: (k_yn, k_oz), 3: (k_pz, wx(1)), 4: (k_ym, wx(2)),
+               5: (wx(3),), 6: (k_yo,), 7: (k_poz,)}
 
     def pair(i, _):
         for when, todo in at_pair.items():
@@ -602,6 +617,7 @@
     blocks = lax.axis_size("sp")
     tables = [jnp.asarray(t) for t in rope_tables(blocks)]
     vm = pl.BlockSpec(memory_space=pltpu.VMEM)
+    hbm = pl.BlockSpec(memory_space=pl.ANY)
     args = (
         tokens.reshape(ROWS, D), in_gain.reshape(1, D), w_query_down, w_latent_down, w_rope_key.T,
         query_latent_gain.reshape(1, QR), latent_gain.reshape(1, KR), w_query_up, w_key_up,
@@ -610,7 +626,7 @@
     out = pl.pallas_call(
         kernel,
         out_shape=pltpu.VMEM((ROWS, D), BF),
-        in_specs=[vm] * len(args),
+        in_specs=[hbm if i in (0, 2, 3, 4, 7, 8, 9) or i > 12 else vm for i in range(len(args))],
         out_specs=vm,
         scratch_shapes=[
             pltpu.VMEM((8, 256, QR + KR), BF),
@@ -622,7 +638,7 @@
             pltpu.VMEM((ROWS, QR + KR), F32),
             pltpu.VMEM((LOCAL, QR, 256), BF),
             pltpu.VMEM((LOCAL, NOPE, KR), BF),
-            pltpu.VMEM((LOCAL, KR, VD), BF),
+            pltpu.VMEM((LOCAL // 2, KR, 2 * VD), BF),
             pltpu.VMEM((2, LOCAL, ROWS, 256), BF),
             pltpu.VMEM((KEPT, LOCAL, 256, 256), BF),
             pltpu.VMEM((KEPT, LOCAL, 256, 256), BF),
@@ -633,6 +649,13 @@
             pltpu.VMEM((1, 256), F32),
             pltpu.VMEM((NOPE, 256), F32),
             pltpu.VMEM((ROPE, 256), F32),
+            pltpu.VMEM((ROWS, D), BF),
+            pltpu.VMEM((ROPE, D), BF),
+            pltpu.VMEM((64, QK), BF),
+        ]
+        + [pltpu.VMEM(t.shape, F32) for t in tables]
+        + [
+            pltpu.SemaphoreType.DMA((12,)),
             pltpu.SemaphoreType.DMA((SLOTS,)),
             pltpu.SemaphoreType.DMA((SLOTS,)),
         ],

time: 85.8 us -> 80.1 us (0.934)
  Pallas kernels: 84.7 us -> 79 us
    pallas_call x1, Pallas kernels: 84.7 us -> 79 us  [per_device(): pl.pallas_call(kernel, out_shape=pltpu.VMEM((ROWS, D), BF), in_specs=[hbm...]
where the time goes in v7:
time: 80.1 us; the launch traced here: 80 us
  Pallas kernels  79 us (99%)
  local copies, waits for them, and re-layouts  0.97 us (1%)
    pallas_call x1, Pallas kernels, per_device(): pl.pallas_call(kernel, out_shape=pltpu.VMEM((ROWS, D), BF), in_specs=[hbm...  79 us

profile of v7, /device:TPU:24, one launch (start us, length us, event | category | flops | bytes accessed | tf_op | source)
XLA Modules:
  0.0 80.0 jit_solution(17294167702368158815)
XLA Ops:
  0.0 79.0 %shard_map.172 = bf16[256,2048]{1,0:T(8,128)(2,1)S(1)} custom-call(bf16[256,2048]{1,0:T(8,128)(2,1)} %bitcast.10, f32[1,2048]{1,0:T(1,128)} %bitcast.12, bf16[256,512]{1,0:T(8,128)(2,1)} %wqd_in.1, bf16[256,256]{1,0:T(8,128)(2,1)} %wld_in.1, bf16[64,2048]{1,0:T(8,128)(2,1)} %bitcast.11, f32[1,512]{1,0:T(1,128)} %bitcast.14, f32[1,256]{1,0:T(1,128)} %bitcast.15, ...), custom_call_target="tpu_custom_call" | custom-call | tf_op jit(solution)/shard_map/pallas_call | solution.py:626
  79.0 1.0 %copy.20 = bf16[1,256,2048]{2,1,0:T(8,128)(2,1)} copy(bf16[1,256,2048]{2,1,0:T(8,128)(2,1)S(1)} %bitcast.9) | data formatting | bytes 2097152

commit v8 on v7

--- a/solution.py
+++ b/solution.py
@@ -124,9 +124,13 @@
 
 
 def attend_pair(q_ref, kt_ref, v_ref, m_ref, acc_ref, which):
+    def score(h):
+        q = q_ref[which, h]
+        return dot(q, kt_ref[0, h]), dot(q, kt_ref[1, h])
+
+    s0, s1 = score(0)
     for h in range(LOCAL):
-        q = q_ref[which, h]
-        s0, s1 = dot(q, kt_ref[0, h]), dot(q, kt_ref[1, h])
+        ahead = score(h + 1) if h + 1 < LOCAL else None
         old = m_ref[which, h]
         new = jnp.maximum(old, jnp.max(jnp.maximum(s0, s1), axis=1, keepdims=True))
         fade = jnp.exp2((old - new) * SOFT)
@@ -137,6 +141,8 @@
         acc_ref[which, h] = acc_ref[which, h] * jnp.concatenate([fade, fade], 1) + (
             dot(p0, v_ref[0, h]) + dot(p1, v_ref[1, h])
         )
+        if ahead is not None:
+            s0, s1 = ahead
 
 
 def close_heads(acc_ref, which, att_ref, first):
@@ -538,7 +544,7 @@
     def _():
         attend_pair(q_ref, kt_ref, v_ref, m_ref, acc_ref, 1)
 
-    at_pair = {1: (k_oy, k_zm, wx(0)), 2: (k_yn, k_oz), 3: (k_pz, wx(1)), 4: (k_ym, wx(2)),
+    at_pair = {1: (k_zm, k_oy, wx(0)), 2: (k_yn,), 3: (k_oz, k_pz, wx(1)), 4: (k_ym, wx(2)),
                5: (wx(3),), 6: (k_yo,), 7: (k_poz,)}
 
     def pair(i, _):

time: 80.1 us -> 79.1 us (0.988)
  the two profiles are of different devices: /device:TPU:24 before, /device:TPU:56 now
where the time goes in v8:
time: 79.1 us; the launch traced here: 78.9 us
  Pallas kernels  78 us (99%)
  local copies, waits for them, and re-layouts  0.97 us (1%)
    pallas_call x1, Pallas kernels, per_device(): pl.pallas_call(kernel, out_shape=pltpu.VMEM((ROWS, D), BF), in_specs=[hbm...  78 us

profile of v8, /device:TPU:56, one launch (start us, length us, event | category | flops | bytes accessed | tf_op | source)
XLA Modules:
  0.0 78.9 jit_solution(11591855965927194551)
XLA Ops:
  0.0 78.0 %shard_map.172 = bf16[256,2048]{1,0:T(8,128)(2,1)S(1)} custom-call(bf16[256,2048]{1,0:T(8,128)(2,1)} %bitcast.10, f32[1,2048]{1,0:T(1,128)} %bitcast.12, bf16[256,512]{1,0:T(8,128)(2,1)} %wqd_in.1, bf16[256,256]{1,0:T(8,128)(2,1)} %wld_in.1, bf16[64,2048]{1,0:T(8,128)(2,1)} %bitcast.11, f32[1,512]{1,0:T(1,128)} %bitcast.14, f32[1,256]{1,0:T(1,128)} %bitcast.15, ...), custom_call_target="tpu_custom_call" | custom-call | tf_op jit(solution)/shard_map/pallas_call | solution.py:632
  78.0 1.0 %copy.20 = bf16[1,256,2048]{2,1,0:T(8,128)(2,1)} copy(bf16[1,256,2048]{2,1,0:T(8,128)(2,1)S(1)} %bitcast.9) | data formatting | bytes 2097152

commit v9 on v8

--- a/solution.py
+++ b/solution.py
@@ -81,7 +81,7 @@
         q_ref[which, h, :, NOPE:256] = turned.astype(BF)
 
 
-def expand(unit, block, wkt_ref, wv_ref, gk_ref, gr_ref, lowk_ref, highk_ref, kt_ref, v_ref, slot):
+def expand(unit, block, wkt_ref, wv_ref, gk_ref, gr_ref, lowk_ref, highk_ref, place):
     kv = unit[0:256, :]
     rope = unit[256:320, :].astype(F32)
     half = ROPE // 2
@@ -94,21 +94,23 @@
     x = rope * gr_ref[...]
     a, b = x[0:half], x[half:ROPE]
     turned = jnp.concatenate([a * cosine - b * sine, b * cosine + a * sine], axis=0)
-    kt = dot_nt(wkt_ref[...].reshape(LOCAL * NOPE, KR), kv)
+    keys = dot_nt(wkt_ref[...].reshape(LOCAL * NOPE, KR), kv)
     for h in range(LOCAL):
-        k = kt[h * NOPE : (h + 1) * NOPE]
+        k = keys[h * NOPE : (h + 1) * NOPE]
         scale = lax.rsqrt((jnp.sum(k * k, axis=0, keepdims=True) + rope_sq) * (1.0 / QK) + EPS)
-        kt_ref[slot, h, 0:NOPE] = (k * scale * gk_ref[...]).astype(BF)
-        kt_ref[slot, h, NOPE:QK] = (turned * scale).astype(BF)
+        kt, _ = place(h)
+        kt[0:NOPE] = (k * scale * gk_ref[...]).astype(BF)
+        kt[NOPE:QK] = (turned * scale).astype(BF)
     for h in range(0, LOCAL, 2):
         v = dot(kv, wv_ref[h // 2]).astype(BF)
-        v_ref[slot, h, :, 0:VD] = v[:, 0:VD]
-        v_ref[slot, h + 1, :, 0:VD] = v[:, VD : 2 * VD]
-
-
-def attend(diagonal, q_ref, kt_ref, v_ref, m_ref, acc_ref, which, slot):
+        place(h)[1][:, 0:VD] = v[:, 0:VD]
+        place(h + 1)[1][:, 0:VD] = v[:, VD : 2 * VD]
+
+
+def attend(diagonal, q_ref, place, m_ref, acc_ref, which):
     for h in range(LOCAL):
-        s = dot(q_ref[which, h], kt_ref[slot, h])
+        kt, v = place(h)
+        s = dot(q_ref[which, h], kt[...])
         if diagonal:
             row = lax.broadcasted_iota(jnp.int32, (ROWS, ROWS), 0)
             col = lax.broadcasted_iota(jnp.int32, (ROWS, ROWS), 1)
@@ -119,18 +121,18 @@
         p = jnp.exp2((s - jnp.concatenate([new, new], 1)) * SOFT).astype(BF)
         m_ref[which, h] = new
         acc_ref[which, h] = acc_ref[which, h] * jnp.concatenate([fade, fade], 1) + dot(
-            p, v_ref[slot, h]
+            p, v[...]
         )
 
 
-def attend_pair(q_ref, kt_ref, v_ref, m_ref, acc_ref, which):
+def attend_pair(q_ref, place0, place1, m_ref, acc_ref, which, heads):
     def score(h):
         q = q_ref[which, h]
-        return dot(q, kt_ref[0, h]), dot(q, kt_ref[1, h])
-
-    s0, s1 = score(0)
-    for h in range(LOCAL):
-        ahead = score(h + 1) if h + 1 < LOCAL else None
+        return dot(q, place0(h)[0][...]), dot(q, place1(h)[0][...])
+
+    s0, s1 = score(heads[0])
+    for h in heads:
+        ahead = score(h + 1) if h + 1 in heads else None
         old = m_ref[which, h]
         new = jnp.maximum(old, jnp.max(jnp.maximum(s0, s1), axis=1, keepdims=True))
         fade = jnp.exp2((old - new) * SOFT)
@@ -139,14 +141,14 @@
         p1 = jnp.exp2((s1 - wide) * SOFT).astype(BF)
         m_ref[which, h] = new
         acc_ref[which, h] = acc_ref[which, h] * jnp.concatenate([fade, fade], 1) + (
-            dot(p0, v_ref[0, h]) + dot(p1, v_ref[1, h])
+            dot(p0, place0(h)[1][...]) + dot(p1, place1(h)[1][...])
         )
         if ahead is not None:
             s0, s1 = ahead
 
 
-def close_heads(acc_ref, which, att_ref, first):
-    for h in range(LOCAL):
+def close_heads(acc_ref, which, att_ref, first, heads=range(LOCAL)):
+    for h in heads:
         att_ref[first + h] = (
             acc_ref[which, h, :, 0:VD] / acc_ref[which, h, :, VD : 2 * VD]
         ).astype(BF)
@@ -176,14 +178,14 @@
 
 
 SLOTS = 128
-KEPT = 2
+SPLIT = 4
 
 
 def kernel(
     tok_in, ing_ref, wqd_in, wld_in, wrt_in, qlg_ref, klg_ref, wqu_in, wku_in, wvu_in,
     qg_ref, kg_ref, ogain_ref, wo_in, lowq_in, highq_in, lowk_in, highk_in,
     out_ref,
-    wd, us, wo, kvb, lq, normed, sums, wq_ref, wkt_ref, wv_ref, q_ref, kt_ref, v_ref,
+    wd, us, wo, kvb, lq, normed, sums, wq_ref, wkt_ref, wv_ref, q_ref, kt_ref, v_ref, kt_keep, v_keep,
     m_ref, acc_ref, att_ref, mixed_ref, qgain_ref, gk_ref, gr_ref,
     tok_ref, wrt_ref, wqu_ref, lowq_ref, highq_ref, lowk_ref, highk_ref, lsem, ssem, rsem,
 ):
@@ -313,8 +315,15 @@
     m_ref[...] = jnp.full(m_ref.shape, NEG_BIG, F32)
     acc_ref[...] = jnp.zeros(acc_ref.shape, F32)
     wq_ref[:, :, QK:256] = jnp.zeros((LOCAL, QR, 256 - QK), BF)
-    kt_ref[:, :, QK:256, :] = jnp.zeros((KEPT, LOCAL, 256 - QK, 256), BF)
-    v_ref[:, :, :, VD:256] = jnp.ones((KEPT, LOCAL, ROWS, 256 - VD), BF)
+    kt_ref[:, :, QK:256, :] = jnp.zeros((2, SPLIT, 256 - QK, 256), BF)
+    v_ref[:, :, :, VD:256] = jnp.ones((2, SPLIT, ROWS, 256 - VD), BF)
+
+    def blank(i, _):
+        kt_keep[i, :, QK:256, :] = jnp.zeros((LOCAL - SPLIT, 256 - QK, 256), BF)
+        v_keep[i, :, :, VD:256] = jnp.ones((LOCAL - SPLIT, ROWS, 256 - VD), BF)
+        return 0
+
+    lax.fori_loop(0, 16, blank, 0)
     rope_t = jnp.zeros((ROPE, ROWS), F32)
     for k in range(8):
         rope_t = rope_t + dot_nt(wrt_ref[:, k * 256 : (k + 1) * 256], normed[k])
@@ -481,9 +490,22 @@
     hfirst = (z // 2) * LOCAL
     b_own, b_mate = sp, zmate * 4 + y
 
-    def send_mate():
-        close_heads(acc_ref, 1, att_ref, HEADS)
-        push("att", lambda: att_ref.at[HEADS : HEADS + LOCAL], dev(zz=zmate), att_ref.at[pl.ds(hfirst, LOCAL)])
+    low, high = range(SPLIT), range(SPLIT, LOCAL)
+
+    def send_mate(heads):
+        close_heads(acc_ref, 1, att_ref, HEADS, heads)
+        push(
+            f"att{heads[0]}", lambda: att_ref.at[HEADS + heads[0] : HEADS + heads[-1] + 1],
+            dev(zz=zmate), att_ref.at[pl.ds(hfirst + heads[0], SPLIT)],
+        )
+
+    def place(slot, step):
+        def of(h):
+            if h < SPLIT:
+                return kt_ref.at[slot, h], v_ref.at[slot, h]
+            return kt_keep.at[step, h - SPLIT], v_keep.at[step, h - SPLIT]
+
+        return of
 
     def pick(test, yes, no):
         return no + test.astype(jnp.int32) * (yes - no)
@@ -504,27 +526,33 @@
     def expand_step(step, slot):
         yy, zz, b = source(step)
         expand(
-            kvb[yy, zz], b, wkt_ref, wv_ref, gk_ref, gr_ref, lowk_ref, highk_ref, kt_ref,
-            v_ref, slot,
+            kvb[yy, zz], b, wkt_ref, wv_ref, gk_ref, gr_ref, lowk_ref, highk_ref,
+            place(slot, step),
         )
 
-    def attend_to(which, slot, diagonal=False):
-        attend(diagonal, q_ref, kt_ref, v_ref, m_ref, acc_ref, which, slot)
-
-    def singles(b0, b1, own0, own1, skip_own, skip_mate):
+    def attend_to(which, slot, step, diagonal=False):
+        attend(diagonal, q_ref, place(slot, step), m_ref, acc_ref, which)
+
+    def attend_both(which, first, second, heads):
+        attend_pair(
+            q_ref, place(0, first), place(1, second), m_ref, acc_ref, which, heads
+        )
+
+    def singles(first, second, b0, b1, own0, own1, skip_own, skip_mate):
         def single(j, _):
             which, slot = j // 2, j % 2
+            step = pick(slot == 0, first, second)
             b = pick(slot == 0, b0, b1)
             mine = pick(slot == 0, own0.astype(jnp.int32), own1.astype(jnp.int32)) * (1 - skip_own)
             mates = (b < b_mate).astype(jnp.int32) * (1 - skip_mate)
 
             @pl.when(pick(which == 0, mine, mates) == 1)
             def _():
-                attend_to(which, slot)
+                attend_to(which, slot, step)
 
             @pl.when((b == b_mate) & (which == 1))
             def _():
-                attend_to(which, slot, True)
+                attend_to(which, slot, step, True)
 
             return 0
 
@@ -532,7 +560,7 @@
 
     zero = z - z
     expand_step(zero, 0)
-    attend_to(0, 0, True)
+    attend_to(0, 0, zero, True)
     k_y()
     k_zn()
     expand_step(zero + 1, 0)
@@ -542,7 +570,12 @@
 
     @pl.when(mate_both)
     def _():
-        attend_pair(q_ref, kt_ref, v_ref, m_ref, acc_ref, 1)
+        attend_both(1, zero + 1, zero + 2, low)
+
+    def units(i):
+        first = pick(i == 7, 0, 2 * i + 1)
+        second = pick(i == 7, 15, 2 * i + 2)
+        return first, second, source(first)[2], source(second)[2]
 
     at_pair = {1: (k_zm, k_oy, wx(0)), 2: (k_yn,), 3: (k_oz, k_pz, wx(1)), 4: (k_ym, wx(2)),
                5: (wx(3),), 6: (k_yo,), 7: (k_poz,)}
@@ -554,40 +587,57 @@
                 for f in todo:
                     f()
 
-        first = pick(i == 7, 0, 2 * i + 1)
-        second = pick(i == 7, 15, 2 * i + 2)
-        b0, b1 = source(first)[2], source(second)[2]
+        first, second, b0, b1 = units(i)
         own0 = (b0 < b_own) & (i > 0) & (first > 0)
         own1 = (b1 < b_own) & (i > 0) & (second != 8)
         own_both = own0 & own1
         mate_both = (b0 < b_mate) & (b1 < b_mate)
-        either = (own_both | mate_both) & (i > 0)
         needed = ((b0 <= b_last) | (b1 <= b_last)) & (i > 0)
-        lead = pick(own_both, 0, 1)
-
-        @pl.when(either)
+        mate_first = mate_both & jnp.logical_not(own_both)
+
+        @pl.when(own_both)
         def _():
             expand_step(first, 0)
             expand_step(second, 1)
-            attend_pair(q_ref, kt_ref, v_ref, m_ref, acc_ref, lead)
-
-        @pl.when(jnp.logical_not(either) & needed)
+            attend_both(0, first, second, range(LOCAL))
+
+        @pl.when(mate_first & (i > 0))
         def _():
             expand_step(first, 0)
             expand_step(second, 1)
+            attend_both(1, first, second, low)
+
+        @pl.when(jnp.logical_not(own_both | mate_both) & needed)
+        def _():
+            expand_step(first, 0)
+            expand_step(second, 1)
 
         @pl.when(own_both & mate_both)
         def _():
-            attend_pair(q_ref, kt_ref, v_ref, m_ref, acc_ref, 1)
+            attend_both(1, first, second, low)
 
         @pl.when(jnp.logical_not(own_both & mate_both))
         def _():
-            singles(b0, b1, own0, own1, own_both.astype(jnp.int32), mate_both.astype(jnp.int32))
+            singles(
+                first, second, b0, b1, own0, own1, own_both.astype(jnp.int32), mate_both.astype(jnp.int32),
+            )
 
         return 0
 
     lax.fori_loop(0, 8, pair, 0)
-    send_mate()
+    send_mate(low)
+
+    def rest(i, _):
+        first, second, b0, b1 = units(i)
+
+        @pl.when((b0 < b_mate) & (b1 < b_mate))
+        def _():
+            attend_both(1, first, second, high)
+
+        return 0
+
+    lax.fori_loop(0, 8, rest, 0)
+    send_mate(high)
 
     def last(j, _):
         step = pick(j == 2, 8, j + 1)
@@ -595,7 +645,7 @@
         @pl.when(source(step)[2] < b_own)
         def _():
             expand_step(step, 0)
-            attend_to(0, 0)
+            attend_to(0, 0, step)
 
         return 0
 
@@ -608,7 +658,8 @@
         got(f"w_cl{k}", wo.at[zrow[k], :, xl, co])
         got(f"w_cr{k}", wo.at[zrow[k], :, xr, co])
         got(f"w_co{k}", wo.at[zrow[k], :, xo, co])
-    got("att", att_ref.at[pl.ds(LOCAL - hfirst, LOCAL)])
+    for heads in (low, high):
+        got(f"att{heads[0]}", att_ref.at[pl.ds(LOCAL - hfirst + heads[0], SPLIT)])
     finish(att_ref, mixed_ref, ogain_ref, wo, out_ref)
     for i, again in sent:
         view = again()
@@ -646,8 +697,10 @@
             pltpu.VMEM((LOCAL, NOPE, KR), BF),
             pltpu.VMEM((LOCAL // 2, KR, 2 * VD), BF),
             pltpu.VMEM((2, LOCAL, ROWS, 256), BF),
-            pltpu.VMEM((KEPT, LOCAL, 256, 256), BF),
-            pltpu.VMEM((KEPT, LOCAL, 256, 256), BF),
+            pltpu.VMEM((2, SPLIT, 256, 256), BF),
+            pltpu.VMEM((2, SPLIT, 256, 256), BF),
+            pltpu.VMEM((16, LOCAL - SPLIT, 256, 256), BF),
+            pltpu.VMEM((16, LOCAL - SPLIT, 256, 256), BF),
             pltpu.VMEM((2, LOCAL, ROWS, 128), F32),
             pltpu.VMEM((2, LOCAL, ROWS, 256), F32),
             pltpu.VMEM((HEADS + LOCAL, ROWS, VD), BF),

time: 79.1 us -> 78 us (0.986)
  the two profiles are of different devices: /device:TPU:56 before, /device:TPU:24 now
where the time goes in v9:
time: 78 us; the launch traced here: 77.1 us
  Pallas kernels  76.1 us (98%)
  local copies, waits for them, and re-layouts  0.97 us (1%)
    pallas_call x1, Pallas kernels, per_device(): pl.pallas_call(kernel, out_shape=pltpu.VMEM((ROWS, D), BF), in_specs=[hbm...  76.1 us

profile of v9, /device:TPU:24, one launch (start us, length us, event | category | flops | bytes accessed | tf_op | source)
XLA Modules:
  0.0 77.1 jit_solution(17079662647091618069)
XLA Ops:
  0.0 76.1 %shard_map.172 = bf16[256,2048]{1,0:T(8,128)(2,1)S(1)} custom-call(bf16[256,2048]{1,0:T(8,128)(2,1)} %bitcast.10, f32[1,2048]{1,0:T(1,128)} %bitcast.12, bf16[256,512]{1,0:T(8,128)(2,1)} %wqd_in.1, bf16[256,256]{1,0:T(8,128)(2,1)} %wld_in.1, bf16[64,2048]{1,0:T(8,128)(2,1)} %bitcast.11, f32[1,512]{1,0:T(1,128)} %bitcast.14, f32[1,256]{1,0:T(1,128)} %bitcast.15, ...), custom_call_target="tpu_custom_call" | custom-call | tf_op jit(solution)/shard_map/pallas_call | solution.py:683
  76.1 1.0 %copy.20 = bf16[1,256,2048]{2,1,0:T(8,128)(2,1)} copy(bf16[1,256,2048]{2,1,0:T(8,128)(2,1)S(1)} %bitcast.9) | data formatting | bytes 2097152

commit v10 on v9

--- a/solution.py
+++ b/solution.py
@@ -485,7 +485,7 @@
         r = zrow[k]
         got(f"w_oxr{k}", wo.at[r, 0:2, xo, c])
         got(f"w_oxl{k}", wo.at[r, 2:4, xo, c])
-        push(f"w_co{k}", wo.at[r, :, xo, c], CORE)
+        push(f"w_co{k}", lambda: wo.at[r, :, xo, c], CORE)
 
     hfirst = (z // 2) * LOCAL
     b_own, b_mate = sp, zmate * 4 + y
@@ -578,7 +578,18 @@
         return first, second, source(first)[2], source(second)[2]
 
     at_pair = {1: (k_zm, k_oy, wx(0)), 2: (k_yn,), 3: (k_oz, k_pz, wx(1)), 4: (k_ym, wx(2)),
-               5: (wx(3),), 6: (k_yo,), 7: (k_poz,)}
+               5: (wx(3),), 6: (k_yo,), 7: (k_poz, lambda: wxo(0), lambda: wxo(1))}
+    i_send = pick(z == 3, 6, 8)
+
+    def rest(i, _):
+        first, second, b0, b1 = units(i)
+
+        @pl.when((b0 < b_mate) & (b1 < b_mate))
+        def _():
+            attend_both(1, first, second, high)
+
+        return 0
+
 
     def pair(i, _):
         for when, todo in at_pair.items():
@@ -587,6 +598,19 @@
                 for f in todo:
                     f()
 
+        @pl.when(i == i_send)
+        def _():
+            send_mate(low)
+            lax.fori_loop(0, 8, rest, 0)
+            send_mate(high)
+
+        @pl.when(i < 8)
+        def _():
+            pair_work(i)
+
+        return 0
+
+    def pair_work(i):
         first, second, b0, b1 = units(i)
         own0 = (b0 < b_own) & (i > 0) & (first > 0)
         own1 = (b1 < b_own) & (i > 0) & (second != 8)
@@ -622,22 +646,9 @@
                 first, second, b0, b1, own0, own1, own_both.astype(jnp.int32), mate_both.astype(jnp.int32),
             )
 
-        return 0
-
-    lax.fori_loop(0, 8, pair, 0)
-    send_mate(low)
-
-    def rest(i, _):
-        first, second, b0, b1 = units(i)
-
-        @pl.when((b0 < b_mate) & (b1 < b_mate))
-        def _():
-            attend_both(1, first, second, high)
-
-        return 0
-
-    lax.fori_loop(0, 8, rest, 0)
-    send_mate(high)
+    lax.fori_loop(0, 9, pair, 0)
+    for k in (2, 3):
+        wxo(k)
 
     def last(j, _):
         step = pick(j == 2, 8, j + 1)
@@ -651,8 +662,6 @@
 
     lax.fori_loop(0, 3, last, 0)
     close_heads(acc_ref, 0, att_ref, hfirst)
-    for k in range(4):
-        wxo(k)
     got("w_c", wo.at[:, :, x, co])
     for k in range(4):
         got(f"w_cl{k}", wo.at[zrow[k], :, xl, co])

time: 78 us -> 78.2 us (level)
  the two profiles are of different devices: /device:TPU:24 before, /device:TPU:48 now
where the time goes in v10:
time: 78.2 us; the launch traced here: 78.1 us
  Pallas kernels  77.1 us (99%)
  local copies, waits for them, and re-layouts  0.97 us (1%)
    pallas_call x1, Pallas kernels, per_device(): pl.pallas_call(kernel, out_shape=pltpu.VMEM((ROWS, D), BF), in_specs=[hbm...  77.1 us

profile of v10, /device:TPU:48, one launch (start us, length us, event | category | flops | bytes accessed | tf_op | source)
XLA Modules:
  0.0 78.1 jit_solution(3699834519823455589)
XLA Ops:
  0.0 77.1 %shard_map.172 = bf16[256,2048]{1,0:T(8,128)(2,1)S(1)} custom-call(bf16[256,2048]{1,0:T(8,128)(2,1)} %bitcast.10, f32[1,2048]{1,0:T(1,128)} %bitcast.12, bf16[256,512]{1,0:T(8,128)(2,1)} %wqd_in.1, bf16[256,256]{1,0:T(8,128)(2,1)} %wld_in.1, bf16[64,2048]{1,0:T(8,128)(2,1)} %bitcast.11, f32[1,512]{1,0:T(1,128)} %bitcast.14, f32[1,256]{1,0:T(1,128)} %bitcast.15, ...), custom_call_target="tpu_custom_call" | custom-call | tf_op jit(solution)/shard_map/pallas_call | solution.py:692
  77.1 1.0 %copy.20 = bf16[1,256,2048]{2,1,0:T(8,128)(2,1)} copy(bf16[1,256,2048]{2,1,0:T(8,128)(2,1)S(1)} %bitcast.9) | data formatting | bytes 2097152

commit v11 on v10

--- a/solution.py
+++ b/solution.py
@@ -577,7 +577,7 @@
         second = pick(i == 7, 15, 2 * i + 2)
         return first, second, source(first)[2], source(second)[2]
 
-    at_pair = {1: (k_zm, k_oy, wx(0)), 2: (k_yn,), 3: (k_oz, k_pz, wx(1)), 4: (k_ym, wx(2)),
+    at_pair = {1: (k_zm, k_oy, wx(0)), 2: (k_yn,), 3: (k_oz, wx(1)), 4: (k_ym, k_pz, wx(2)),
                5: (wx(3),), 6: (k_yo,), 7: (k_poz, lambda: wxo(0), lambda: wxo(1))}
     i_send = pick(z == 3, 6, 8)
 
@@ -612,8 +612,9 @@
 
     def pair_work(i):
         first, second, b0, b1 = units(i)
-        own0 = (b0 < b_own) & (i > 0) & (first > 0)
-        own1 = (b1 < b_own) & (i > 0) & (second != 8)
+        now = (i > 0) & jnp.logical_not((z == 2) & (i > 5))
+        own0 = (b0 < b_own) & now & (first > 0)
+        own1 = (b1 < b_own) & now & (second != 8)
         own_both = own0 & own1
         mate_both = (b0 < b_mate) & (b1 < b_mate)
         needed = ((b0 <= b_last) | (b1 <= b_last)) & (i > 0)
@@ -651,16 +652,16 @@
         wxo(k)
 
     def last(j, _):
-        step = pick(j == 2, 8, j + 1)
-
-        @pl.when(source(step)[2] < b_own)
+        step = pick(j == 2, 8, pick(j < 2, j + 1, j + 10))
+
+        @pl.when((source(step)[2] < b_own) & ((j < 3) | (z == 2)))
         def _():
             expand_step(step, 0)
             attend_to(0, 0, step)
 
         return 0
 
-    lax.fori_loop(0, 3, last, 0)
+    lax.fori_loop(0, 6, last, 0)
     close_heads(acc_ref, 0, att_ref, hfirst)
     got("w_c", wo.at[:, :, x, co])
     for k in range(4):

time: 78.2 us -> 73 us (0.934)
  the two profiles are of different devices: /device:TPU:48 before, /device:TPU:24 now
where the time goes in v11:
time: 73 us; the launch traced here: 72.4 us
  Pallas kernels  71.4 us (98%)
  local copies, waits for them, and re-layouts  0.97 us (1%)
    pallas_call x1, Pallas kernels, per_device(): pl.pallas_call(kernel, out_shape=pltpu.VMEM((ROWS, D), BF), in_specs=[hbm...  71.4 us

profile of v11, /device:TPU:24, one launch (start us, length us, event | category | flops | bytes accessed | tf_op | source)
XLA Modules:
  0.0 72.4 jit_solution(8952513922256064742)
XLA Ops:
  0.0 71.4 %shard_map.172 = bf16[256,2048]{1,0:T(8,128)(2,1)S(1)} custom-call(bf16[256,2048]{1,0:T(8,128)(2,1)} %bitcast.10, f32[1,2048]{1,0:T(1,128)} %bitcast.12, bf16[256,512]{1,0:T(8,128)(2,1)} %wqd_in.1, bf16[256,256]{1,0:T(8,128)(2,1)} %wld_in.1, bf16[64,2048]{1,0:T(8,128)(2,1)} %bitcast.11, f32[1,512]{1,0:T(1,128)} %bitcast.14, f32[1,256]{1,0:T(1,128)} %bitcast.15, ...), custom_call_target="tpu_custom_call" | custom-call | tf_op jit(solution)/shard_map/pallas_call | solution.py:693
  71.4 1.0 %copy.20 = bf16[1,256,2048]{2,1,0:T(8,128)(2,1)} copy(bf16[1,256,2048]{2,1,0:T(8,128)(2,1)S(1)} %bitcast.9) | data formatting | bytes 2097152

commit v12 on v11

--- a/solution.py
+++ b/solution.py
@@ -58,7 +58,7 @@
     wkt_ref[h] = jnp.concatenate(keys, axis=0).T
 
 
-def make_queries(latq, block, wq_ref, qgain, lowq_ref, highq_ref, q_ref, which):
+def make_queries(latq, block, wq_ref, qgain, lowq_ref, highq_ref, q_ref, which, heads):
     ch, sh = highq_ref[block, 0, 0:1], highq_ref[block, 1, 0:1]
     cl, sl = lowq_ref[0], lowq_ref[1]
     cosine = ch * cl - sh * sl
@@ -67,7 +67,7 @@
     sine_a = jnp.where(lane < ROPE // 2, -sine, 0.0)
     sine_b = jnp.where(lane < ROPE // 2, 0.0, sine)
 
-    for h in range(LOCAL):
+    for h in heads:
         q = dot(latq, wq_ref[h])
         scale = lax.rsqrt(jnp.sum(q * q, axis=1, keepdims=True) * (1.0 / QK) + EPS)
         n = q * scale * qgain
@@ -154,11 +154,15 @@
         ).astype(BF)
 
 
-def finish(att_ref, mixed_ref, ogain_ref, wo_ref, out_ref):
+def squares(att_ref, first, count):
     total = jnp.zeros((ROWS, VD), F32)
-    for h in range(HEADS):
-        at = att_ref[h].astype(F32)
+    for h in range(count):
+        at = att_ref[first + h].astype(F32)
         total = total + at * at
+    return total
+
+
+def finish(att_ref, total, mixed_ref, ogain_ref, wo_ref, out_ref):
     scale = lax.rsqrt(jnp.sum(total, axis=1, keepdims=True) * (1.0 / (HEADS * VD)) + EPS)
     for h in range(HEADS):
         cols = slice(h * VD, (h + 1) * VD)
@@ -396,6 +400,11 @@
     push("k_zn", own, Z_N)
     push("k_zm", own, Z_M)
 
+    def queries_own(heads):
+        make_queries(lq[0], sp, wq_ref, qgain_ref[...], lowq_ref, highq_ref, q_ref, 0, heads)
+
+    queries_own((base0 + y, base1 + y, base0 + yl, base0 + yr))
+
     for j, base in ((0, base0), (1, base1)):
         got(f"u_y{j}or", us.at[c, base + yo, 0:2])
         got(f"u_y{j}ol", us.at[c, base + yo, 2:4])
@@ -410,7 +419,7 @@
     push("w_c", wo.at[:, :, x, c], CORE)
     for h in (base0 + yo, base1 + yl, base1 + yr, base1 + yo):
         prepare_head(us, h, wq_ref, wkt_ref, wv_ref)
-    make_queries(lq[0], sp, wq_ref, qgain_ref[...], lowq_ref, highq_ref, q_ref, 0)
+    queries_own((base0 + yo, base1 + yl, base1 + yr, base1 + yo))
     def k_y():
         got("k_yr", kvb.at[yl, z])
         push("k_oyr", lambda: kvb.at[yl, z, 0:160], Y_R)
@@ -466,7 +475,8 @@
     def queries_mate():
         got("q", lq.at[1])
         make_queries(
-            lq[1], zmate * 4 + y, wq_ref, qgain_ref[...], lowq_ref, highq_ref, q_ref, 1
+            lq[1], zmate * 4 + y, wq_ref, qgain_ref[...], lowq_ref, highq_ref, q_ref, 1,
+            range(LOCAL),
         )
 
     def wx(k):
@@ -668,9 +678,12 @@
         got(f"w_cl{k}", wo.at[zrow[k], :, xl, co])
         got(f"w_cr{k}", wo.at[zrow[k], :, xr, co])
         got(f"w_co{k}", wo.at[zrow[k], :, xo, co])
+    total = squares(att_ref, hfirst, LOCAL)
     for heads in (low, high):
-        got(f"att{heads[0]}", att_ref.at[pl.ds(LOCAL - hfirst + heads[0], SPLIT)])
-    finish(att_ref, mixed_ref, ogain_ref, wo, out_ref)
+        first = LOCAL - hfirst + heads[0]
+        got(f"att{heads[0]}", att_ref.at[pl.ds(first, SPLIT)])
+        total = total + squares(att_ref, first, SPLIT)
+    finish(att_ref, total, mixed_ref, ogain_ref, wo, out_ref)
     for i, again in sent:
         view = again()
         pltpu.make_async_copy(view, view, ssem.at[i]).wait()

time: 73 us -> 72.9 us (level)
  no operation moved by 1% of the time
where the time goes in v12:
time: 72.9 us; the launch traced here: 72.3 us
  Pallas kernels  71.3 us (98%)
  local copies, waits for them, and re-layouts  0.97 us (1%)
    pallas_call x1, Pallas kernels, per_device(): pl.pallas_call(kernel, out_shape=pltpu.VMEM((ROWS, D), BF), in_specs=[hbm...  71.3 us

profile of v12, /device:TPU:24, one launch (start us, length us, event | category | flops | bytes accessed | tf_op | source)
XLA Modules:
  0.0 72.3 jit_solution(17523590403127309230)
XLA Ops:
  0.0 71.3 %shard_map.172 = bf16[256,2048]{1,0:T(8,128)(2,1)S(1)} custom-call(bf16[256,2048]{1,0:T(8,128)(2,1)} %bitcast.10, f32[1,2048]{1,0:T(1,128)} %bitcast.12, bf16[256,512]{1,0:T(8,128)(2,1)} %wqd_in.1, bf16[256,256]{1,0:T(8,128)(2,1)} %wld_in.1, bf16[64,2048]{1,0:T(8,128)(2,1)} %bitcast.11, f32[1,512]{1,0:T(1,128)} %bitcast.14, f32[1,256]{1,0:T(1,128)} %bitcast.15, ...), custom_call_target="tpu_custom_call" | custom-call | tf_op jit(solution)/shard_map/pallas_call | solution.py:706
  71.4 1.0 %copy.20 = bf16[1,256,2048]{2,1,0:T(8,128)(2,1)} copy(bf16[1,256,2048]{2,1,0:T(8,128)(2,1)S(1)} %bitcast.9) | data formatting | bytes 2097152

commit v13 on v12

--- a/solution.py
+++ b/solution.py
@@ -81,7 +81,7 @@
         q_ref[which, h, :, NOPE:256] = turned.astype(BF)
 
 
-def expand(unit, block, wkt_ref, wv_ref, gk_ref, gr_ref, lowk_ref, highk_ref, place):
+def expand(unit, block, wkt_ref, wv_ref, gk_ref, gr_ref, lowk_ref, highk_ref, place, count):
     kv = unit[0:256, :]
     rope = unit[256:320, :].astype(F32)
     half = ROPE // 2
@@ -94,14 +94,14 @@
     x = rope * gr_ref[...]
     a, b = x[0:half], x[half:ROPE]
     turned = jnp.concatenate([a * cosine - b * sine, b * cosine + a * sine], axis=0)
-    keys = dot_nt(wkt_ref[...].reshape(LOCAL * NOPE, KR), kv)
-    for h in range(LOCAL):
+    keys = dot_nt(wkt_ref[0:count].reshape(count * NOPE, KR), kv)
+    for h in range(count):
         k = keys[h * NOPE : (h + 1) * NOPE]
         scale = lax.rsqrt((jnp.sum(k * k, axis=0, keepdims=True) + rope_sq) * (1.0 / QK) + EPS)
         kt, _ = place(h)
         kt[0:NOPE] = (k * scale * gk_ref[...]).astype(BF)
         kt[NOPE:QK] = (turned * scale).astype(BF)
-    for h in range(0, LOCAL, 2):
+    for h in range(0, count, 2):
         v = dot(kv, wv_ref[h // 2]).astype(BF)
         place(h)[1][:, 0:VD] = v[:, 0:VD]
         place(h + 1)[1][:, 0:VD] = v[:, VD : 2 * VD]
@@ -533,11 +533,11 @@
 
     b_last = jnp.maximum(b_own, b_mate)
 
-    def expand_step(step, slot):
+    def expand_step(step, slot, count=LOCAL):
         yy, zz, b = source(step)
         expand(
             kvb[yy, zz], b, wkt_ref, wv_ref, gk_ref, gr_ref, lowk_ref, highk_ref,
-            place(slot, step),
+            place(slot, step), count,
         )
 
     def attend_to(which, slot, step, diagonal=False):
@@ -666,7 +666,7 @@
 
         @pl.when((source(step)[2] < b_own) & ((j < 3) | (z == 2)))
         def _():
-            expand_step(step, 0)
+            expand_step(step, 0, SPLIT)
             attend_to(0, 0, step)
 
         return 0

time: 72.9 us -> 72.9 us (level)
  no operation moved by 1% of the time
where the time goes in v13:
time: 72.9 us; the launch traced here: 72.3 us
  Pallas kernels  71.3 us (98%)
  local copies, waits for them, and re-layouts  0.97 us (1%)
    pallas_call x1, Pallas kernels, per_device(): pl.pallas_call(kernel, out_shape=pltpu.VMEM((ROWS, D), BF), in_specs=[hbm...  71.3 us

profile of v13, /device:TPU:24, one launch (start us, length us, event | category | flops | bytes accessed | tf_op | source)
XLA Modules:
  0.0 72.3 jit_solution(12574401471862186602)
XLA Ops:
  0.0 71.3 %shard_map.172 = bf16[256,2048]{1,0:T(8,128)(2,1)S(1)} custom-call(bf16[256,2048]{1,0:T(8,128)(2,1)} %bitcast.10, f32[1,2048]{1,0:T(1,128)} %bitcast.12, bf16[256,512]{1,0:T(8,128)(2,1)} %wqd_in.1, bf16[256,256]{1,0:T(8,128)(2,1)} %wld_in.1, bf16[64,2048]{1,0:T(8,128)(2,1)} %bitcast.11, f32[1,512]{1,0:T(1,128)} %bitcast.14, f32[1,256]{1,0:T(1,128)} %bitcast.15, ...), custom_call_target="tpu_custom_call" | custom-call | tf_op jit(solution)/shard_map/pallas_call | solution.py:706
  71.4 1.0 %copy.20 = bf16[1,256,2048]{2,1,0:T(8,128)(2,1)} copy(bf16[1,256,2048]{2,1,0:T(8,128)(2,1)S(1)} %bitcast.9) | data formatting | bytes 2097152
